TPU v7x, 256 devices: a whole 4x4x8 slice. The times are simulated.
256 devices in a mesh: fs: 32 (over z, x), tp: 8 (over y, core).
Axes of the slice: x: 4, y: 4, z: 8, core: 2. Of those that a mesh axis runs over, the one named last changes fastest.
Arguments:
- tokens: bfloat16 [6144, 2048], P('fs'), may hold values from -6 to 6
- norm_gain: float32 [2048], P('fs'), may hold values from 0.1 to 1.9
- expert_gate: float32 [64, 2048, 1024], P(None, 'fs', 'tp'), may hold values from -0.125 to 0.125
- expert_up: float32 [64, 2048, 1024], P(None, 'fs', 'tp'), may hold values from -0.125 to 0.125
- expert_down: float32 [64, 1024, 2048], P(None, 'fs', 'tp'), may hold values from -0.1875 to 0.1875
- shared_gate: float32 [2048, 1024], P('fs', 'tp'), may hold values from -0.125 to 0.125
- shared_up: float32 [2048, 1024], P('fs', 'tp'), may hold values from -0.125 to 0.125
- shared_down: float32 [1024, 2048], P('fs', 'tp'), may hold values from -0.1875 to 0.1875
- expert_ids: int32 [6144, 8], P('fs'), may hold values from 0 to 63, all different within a row; in each aligned block of 192 rows (0 to 191, 192 to 383, ...) at most 48 rows name the same one
- route_weights: float32 [6144, 8], P('fs'), may hold values from 0.25 to 1
Outputs:
- gate_ready: bfloat16 [64, 2048, 1024], P('fs', None, 'tp')
- up_ready: bfloat16 [64, 2048, 1024], P('fs', None, 'tp')
- down_ready: bfloat16 [64, 1024, 2048], P('fs', None, 'tp')
- shared_gate_ready: bfloat16 [2048, 1024], P(None, 'tp')
- shared_up_ready: bfloat16 [2048, 1024], P(None, 'tp')
- shared_down_ready: bfloat16 [1024, 2048], P(None, 'tp')
- mixed: bfloat16 [6144, 2048], P('fs', 'tp')
Inputs may be any that keep to these rules, and one draw needn't show every extreme that they name: `expert_ids`: each row names 8 different experts. Among the 192 rows of one index of fs no expert is named more than 48 times, and in every draw some expert is named exactly 48 times there.
All inputs are finite; a program needn't handle non-finite values.
Results may differ from a plain program's by a relative error of at most 0.0085.
Values may be sent and summed in bfloat16 or wider, within the bound.
A program may use at most 128 MiB of HBM per device.

v0:
```python
import jax
import jax.numpy as jnp
from jax import lax
from jax.sharding import PartitionSpec as P

TOP_K = 8


EPS = 1e-06


def cut_along(shard, dim, size):
    before, after = (shard.shape[:dim], shard.shape[dim + 1 :])
    return jnp.moveaxis(shard.reshape(*before, size, -1, *after), dim, 0)


def piece_ends(length, count):
    turn = length // count
    if turn >= 8:
        turn -= turn % 8
    return [turn * k for k in range(1, count)]


def in_order(parts, dim):
    parts = jnp.moveaxis(parts, 0, dim)
    shape = parts.shape
    return parts.reshape(*shape[:dim], shape[dim] * shape[dim + 1], *shape[dim + 2 :])


def several_exchanges(shard, axis, pieces, split_dim, concat_dim):
    parts = cut_along(shard, split_dim, lax.axis_size(axis))
    split_at = max(range(1, max(2, parts.ndim - 1)), key=lambda d: parts.shape[d])
    done = []
    for share in jnp.split(parts, piece_ends(parts.shape[split_at], pieces), axis=split_at):
        if share.size:
            done.append(lax.all_to_all(share, axis, split_axis=0, concat_axis=0, tiled=True))
    return in_order(jnp.concatenate(done, axis=split_at), concat_dim)


def side_by_side(arrays, axis, dim, along):
    ends, at = ([], 0)
    for a in arrays[:-1]:
        at += a.shape[along]
        ends.append(at)
    both = jnp.concatenate(arrays, axis=along)
    return tuple(jnp.split(lax.all_gather(both, axis, axis=dim, tiled=True), ends, axis=along))


def turned_gather(arrays, axis, dims):
    turned = [jnp.moveaxis(a, dim, 0) for a, dim in zip(arrays, dims)]
    widths = [t[0].size for t in turned]
    both = jnp.concatenate([t.reshape(-1, w) for t, w in zip(turned, widths)], axis=1)
    result = lax.all_gather(both, axis, axis=0, tiled=True)
    parts = jnp.split(result, [sum(widths[:k]) for k in range(1, len(widths))], axis=1)
    return tuple(
        (
            jnp.moveaxis(b.reshape(-1, *t.shape[1:]), 0, dim)
            for b, t, dim in zip(parts, turned, dims)
        )
    )


def expert_hidden(rows, gate_new, up_new):
    first = jnp.einsum("secn,enf->secf", rows, gate_new, preferred_element_type=jnp.float32)
    second = jnp.einsum("secn,enf->secf", rows, up_new, preferred_element_type=jnp.float32)
    return (jax.nn.silu(first) * second).astype(jnp.bfloat16)


def body(
    tokens,
    norm_gain,
    expert_gate,
    expert_up,
    expert_down,
    shared_gate,
    shared_up,
    shared_down,
    expert_ids,
    route_weights,
):
    groups = lax.axis_size("fs")
    experts = expert_gate.shape[0]
    per_group = experts // groups
    tok_count = tokens.shape[0]
    capacity = 2 * tok_count * TOP_K // experts
    gate_local = (expert_gate * norm_gain[None, :, None]).astype(jnp.bfloat16)
    up_local = (expert_up * norm_gain[None, :, None]).astype(jnp.bfloat16)
    down_local = expert_down.astype(jnp.bfloat16)
    gate_local = gate_local.reshape((groups, per_group) + gate_local.shape[1:])
    up_local = up_local.reshape((groups, per_group) + up_local.shape[1:])
    down_local = down_local.reshape((groups, per_group) + down_local.shape[1:])
    shared_first_local = (shared_gate * norm_gain[:, None]).astype(jnp.bfloat16)
    shared_second_local = (shared_up * norm_gain[:, None]).astype(jnp.bfloat16)
    shared_third_local = shared_down.astype(jnp.bfloat16)
    gate_moved, up_moved = (
        several_exchanges(gate_local, "fs", 2, 0, 2),
        several_exchanges(up_local, "fs", 2, 0, 2),
    )
    gate_ready = gate_moved[0]
    up_ready = up_moved[0]
    shared_gate_ready, shared_up_ready, shared_down_ready = (
        *side_by_side((shared_first_local, shared_second_local), "fs", 0, 1),
        lax.all_gather(shared_third_local, "fs", axis=0, tiled=True),
    )
    wide = tokens.astype(jnp.float32)
    normed = (wide * lax.rsqrt(jnp.mean(wide * wide, axis=-1, keepdims=True) + EPS)).astype(
        jnp.bfloat16
    )
    chosen = expert_ids.reshape(-1)
    onehot = (chosen[:, None] == jnp.arange(experts, dtype=jnp.int32)[None, :]).astype(jnp.int32)
    ranks = jnp.sum(jnp.cumsum(onehot, axis=0) * onehot, axis=1) - 1
    owners = jnp.arange(tok_count * TOP_K, dtype=jnp.int32) // TOP_K
    slot_token = jnp.zeros((experts, capacity), jnp.int32).at[chosen, ranks].set(owners)
    outgoing = normed[slot_token.reshape(-1)].reshape(groups, per_group, capacity, normed.shape[1])
    share = capacity // lax.axis_size("tp")
    mine = lax.dynamic_slice_in_dim(outgoing, lax.axis_index("tp") * share, share, 2)
    arrived = lax.all_to_all(mine, "fs", split_axis=0, concat_axis=0, tiled=True)
    hidden = expert_hidden(lax.all_gather(arrived, "tp", axis=2, tiled=True), gate_ready, up_ready)
    shared_first = jnp.dot(normed, shared_gate_ready, preferred_element_type=jnp.float32)
    shared_second = jnp.dot(normed, shared_up_ready, preferred_element_type=jnp.float32)
    shared_hidden = (jax.nn.silu(shared_first) * shared_second).astype(jnp.bfloat16)[None, None]
    down_moved = lax.all_to_all(down_local, "fs", split_axis=0, concat_axis=2, tiled=True)
    down_ready = down_moved[0]
    columns = down_ready.shape[2]
    routed_piece, shared_piece = turned_gather((hidden, shared_hidden), "tp", (3, 3))
    routed_total = jnp.einsum(
        "secf,efd->secd", routed_piece, down_ready, preferred_element_type=jnp.float32
    )
    shared_total = jnp.einsum(
        "abtf,fd->abtd", shared_piece, shared_down_ready, preferred_element_type=jnp.float32
    )
    returned = lax.all_to_all(
        routed_total.astype(jnp.bfloat16), "fs", split_axis=0, concat_axis=0, tiled=True
    )
    returned = returned.reshape(experts * capacity, columns)
    picked = (
        returned[chosen * capacity + ranks].astype(jnp.float32).reshape(tok_count, TOP_K, columns)
    )
    routed = jnp.sum(picked * route_weights[:, :, None], axis=1)
    mixed = (shared_total[0, 0] + routed).astype(jnp.bfloat16)
    return (
        gate_ready,
        up_ready,
        down_ready,
        shared_gate_ready,
        shared_up_ready,
        shared_down_ready,
        mixed,
    )


def solution(mesh):
    in_specs = (
        P("fs", None),
        P("fs"),
        P(None, "fs", "tp"),
        P(None, "fs", "tp"),
        P(None, "fs", "tp"),
        P("fs", "tp"),
        P("fs", "tp"),
        P("fs", "tp"),
        P("fs", None),
        P("fs", None),
    )
    out_specs = (
        P("fs", None, "tp"),
        P("fs", None, "tp"),
        P("fs", None, "tp"),
        P(None, "tp"),
        P(None, "tp"),
        P(None, "tp"),
        P("fs", "tp"),
    )
    return jax.shard_map(body, mesh=mesh, in_specs=in_specs, out_specs=out_specs, check_vma=False)
```

profile of v0, /device:TPU:8, one launch (start us, length us, event | category | flops | bytes accessed | tf_op | source)
XLA Modules:
  0.0 414.2 jit_solution(16375426263147226016)
XLA Ops:
  7.2 0.8 copy.58
  8.4 18.1 %reduce-window.6 = s32[64,12,128]{2,1,0:T(8,128)S(1)} reduce-window(s32[64,12,128]{2,1,0:T(8,128)S(1)} %fusion.25, s32[]{:T(128)} %constant.44.clone.1), window={size=1x1x128 pad=0_0x0_0x127_0}, to_apply=%region_1.0 | reduce-window | flops 12484608 | bytes 786436 | tf_op jit(solution)/shard_map/reduce-window
  26.5 0.2 slice.12
  26.7 0.3 copy.61
  27.1 0.2 broadcast_add_fusion
  27.3 0.1 fusion.27
  27.8 6.2 %scatter_custom_fusion = s32[3072]{0:T(1024)S(1)} fusion(s32[1536]{0:T(1024)S(1)} %get-tuple-element.23, s32[1536]{0:T(1024)S(1)} %get-tuple-element.22, s32[]{:T(128)} %constant.44.clone.1), kind=kCustom, calls=%fused_computation.63 | custom fusion | bytes 12292
  34.3 0.2 fusion.10
  34.5 0.2 fusion.11
  34.7 15.9 %gather_fusion = bf16[3072,2048]{1,0:T(8,128)(2,1)} fusion(bf16[192,2048]{1,0:T(8,128)(2,1)S(1)} %fusion.11, s32[3072]{0:T(1024)S(1)} %broadcast_clamp_fusion), kind=kCustom, calls=%fused_computation | custom fusion | bytes 25178112 | tf_op jit(solution)/shard_map/gather | solution.py:114
  50.7 3.0 constant_dynamic-slice_fusion
  53.7 2.8 copy.64
  56.5 11.4 %all-to-all-start.5 = ((bf16[32,2,6,2048]{3,1,2,0:T(2,128)(2,1)}), bf16[32,2,6,2048]{3,1,2,0:T(2,128)(2,1)S(1)}, u32[]{:S(2)}, u32[]{:S(2)}) async-start(bf16[32,2,6,2048]{3,1,2,0:T(2,128)(2,1)} %copy.64), calls=%async_computation.5 | async-start | bytes 3145728 | tf_op jit(solution)/shard_map/all_to_all | solution.py:117
  68.1 0.6 pad_maximum_fusion.1
  68.8 39.3 %all-to-all-done.5 = bf16[32,2,6,2048]{3,1,2,0:T(2,128)(2,1)S(1)} async-done(((bf16[32,2,6,2048]{3,1,2,0:T(2,128)(2,1)}), bf16[32,2,6,2048]{3,1,2,0:T(2,128)(2,1)S(1)}, u32[]{:S(2)}, u32[]{:S(2)}) %all-to-all-start.5) | async-done | bytes 1572896 | tf_op jit(solution)/shard_map/all_to_all | solution.py:117
  108.1 2.0 copy.65
  110.2 2.8 multiply_convert_fusion
  113.0 0.9 fusion.36
  113.9 24.3 %all_to_all.45 = bf16[32,1,2,32,128]{4,3,2,1,0:T(8,128)(2,1)S(1)} all-to-all(bf16[32,1,2,32,128]{4,3,2,1,0:T(8,128)(2,1)S(1)} %get-tuple-element.11), channel_id=1, replica_groups=mesh['fs'=32,'tp'=8] {'fs'}, dimensions={0} | all-to-all | bytes 1048576 | tf_op jit(solution)/shard_map/all_to_all | solution.py:36
  138.2 3.9 all-to-all-start.1
  142.1 0.9 fusion.35
  143.0 16.5 %all-to-all-done.1 = bf16[32,1,2,32,128]{4,3,2,1,0:T(8,128)(2,1)S(1)} async-done(((bf16[32,1,2,32,128]{4,3,2,1,0:T(8,128)(2,1)}), bf16[32,1,2,32,128]{4,3,2,1,0:T(8,128)(2,1)S(1)}, u32[]{:S(2)}, u32[]{:S(2)}) %all-to-all-start.1) | async-done | bytes 524320 | tf_op jit(solution)/shard_map/all_to_all | solution.py:36
  159.5 20.9 %all_to_all.46 = bf16[32,1,2,32,128]{4,3,2,1,0:T(8,128)(2,1)S(1)} all-to-all(bf16[32,1,2,32,128]{4,3,2,1,0:T(8,128)(2,1)S(1)} %get-tuple-element.9), channel_id=1, replica_groups=mesh['fs'=32,'tp'=8] {'fs'}, dimensions={0} | all-to-all | bytes 1048576 | tf_op jit(solution)/shard_map/all_to_all | solution.py:36
  180.5 4.7 %all-to-all-start.3 = ((bf16[32,1,2,32,128]{4,3,2,1,0:T(8,128)(2,1)}), bf16[32,1,2,32,128]{4,3,2,1,0:T(8,128)(2,1)S(1)}, u32[]{:S(2)}, u32[]{:S(2)}) async-start(bf16[32,1,2,32,128]{4,3,2,1,0:T(8,128)(2,1)} %get-tuple-element.10), calls=%async_computation.3 | async-start | bytes 1048576 | tf_op jit(solution)/shard_map/all_to_all | solution.py:36
  185.1 0.2 all-gather.8.cloned.1.call-start
  185.4 0.1 maximum_bitcast_fusion
  185.6 16.5 %all-to-all-done.3 = bf16[32,1,2,32,128]{4,3,2,1,0:T(8,128)(2,1)S(1)} async-done(((bf16[32,1,2,32,128]{4,3,2,1,0:T(8,128)(2,1)}), bf16[32,1,2,32,128]{4,3,2,1,0:T(8,128)(2,1)S(1)}, u32[]{:S(2)}, u32[]{:S(2)}) %all-to-all-start.3) | async-done | bytes 524320 | tf_op jit(solution)/shard_map/all_to_all | solution.py:36
  202.4 1.7 fusion.34
  204.1 0.4 fusion.37
  204.4 0.4 copy-done.6
  204.8 0.4 fusion.24
  205.2 16.9 %all-gather.6.cloned.1.call-done = bf16[32,2,48,2048]{3,0,1,2:T(8,128)(2,1)} async-done(((bf16[32,2,6,2048]{3,0,1,2:T(8,128)(2,1)}), bf16[32,2,48,2048]{3,0,1,2:T(8,128)(2,1)}) %all-gather.6.cloned.1.call-update) | async-done | bytes 12582928 | tf_op jit(solution)/shard_map/all_gather | solution.py:118
  222.1 18.0 %fusion.2 = f32[2,128,32,48]{1,3,2,0:T(8,128)S(1)} fusion(bf16[2,2048,128,1]{2,1,3,0:T(8,128)(2,1)S(1)} %bitcast.105, bf16[32,2,48,2048]{3,0,1,2:T(8,128)(2,1)} %all-gather.6.cloned.1.call-done), kind=kOutput, calls=%fused_computation.5 | convolution fusion | flops 1610612736 | bytes 15204352 | tf_op jit(solution)/shard_map/secn,enf->secf/dot_general | solution.py:64
  240.2 13.8 %fusion.13 = bf16[128,32,2,48]{0,3,1,2:T(8,128)(2,1)S(1)} fusion(f32[2,128,32,48]{1,3,2,0:T(8,128)S(1)} %fusion.2, bf16[2,2048,128,1]{2,1,3,0:T(8,128)(2,1)S(1)} %bitcast.107, bf16[32,2,48,2048]{3,0,1,2:T(8,128)(2,1)} %all-gather.6.cloned.1.call-done), kind=kOutput, calls=%fused_computation.20 | convolution fusion | flops 1612972032 | bytes 15990784 | tf_op jit(solution)/shard_map/secn,enf->secf/dot_general | solution.py:65
  254.1 0.9 pad_maximum_fusion
  255.0 0.9 copy-done.1
  255.9 0.1 convert_element_type.54
  256.0 38.1 %all_to_all.47 = bf16[32,2,32,256]{3,2,1,0:T(8,128)(2,1)S(1)} all-to-all(bf16[32,2,32,256]{3,2,1,0:T(8,128)(2,1)S(1)} %bitcast.101), channel_id=1, replica_groups=mesh['fs'=32,'tp'=8] {'fs'}, dimensions={0} | all-to-all | bytes 2097152 | tf_op jit(solution)/shard_map/all_to_all | solution.py:122
  294.2 10.5 %all-gather.8.cloned.1.call-done = bf16[1024,3264]{0,1:T(8,128)(2,1)} async-done(((bf16[128,3264]{0,1:T(8,128)(2,1)}), bf16[1024,3264]{0,1:T(8,128)(2,1)}) %all-gather.8.cloned.1.call-update) | async-done | bytes 6684688 | tf_op jit(solution)/shard_map/all_gather | solution.py:53
  304.8 2.8 slice-done
  307.6 1.8 fusion.17
  309.4 1.4 copy.70
  310.8 9.9 %all-to-all-start.6 = ((bf16[32,2,48,256]{3,2,1,0:T(8,128)(2,1)}), bf16[32,2,48,256]{3,2,1,0:T(8,128)(2,1)S(1)}, u32[]{:S(2)}, u32[]{:S(2)}) async-start(bf16[32,2,48,256]{3,2,1,0:T(8,128)(2,1)} %copy.70), calls=%async_computation.6 | async-start | bytes 3145728 | tf_op jit(solution)/shard_map/all_to_all | solution.py:132
  320.9 78.8 %all_gather.13 = bf16[1024,256]{1,0:T(8,128)(2,1)S(1)} all-gather(bf16[32,256]{1,0:T(8,128)(2,1)S(1)} %convert_element_type.57), channel_id=1, replica_groups=mesh['fs'=32,'tp'=8] {'fs'}, dimensions={0}, use_global_device_ids=true | all-gather | bytes 540672 | tf_op jit(solution)/shard_map/all_gather | solution.py:103
  399.7 4.8 %gather_fusion.1 = bf16[1536,256]{1,0:T(8,128)(2,1)S(1)} fusion(bf16[3072,256]{1,0:T(8,128)(2,1)S(1)} %bitcast.96, s32[2048]{0:T(1024)S(1)} %pad_clamp_fusion), kind=kCustom, calls=%fused_computation.1 | custom fusion | bytes 1579008 | tf_op jit(solution)/shard_map/gather | solution.py:137
  404.5 0.5 fusion.12
  405.0 1.9 fusion.22
  406.9 0.8 copy.92
  (60 shorter events, 1.8 us)
Async XLA Ops:
  8.3 19.2 %copy-start.13 = (s32[2]{0:T(128)S(1)}, s32[2]{0:T(128)}, u32[]{:S(2)}) copy-start(s32[2]{0:T(128)} %constant.57) | copy-start | bytes 28
  8.4 19.3 %copy-start.12 = (s32[2]{0:T(128)S(1)}, s32[2]{0:T(128)}, u32[]{:S(2)}) copy-start(s32[2]{0:T(128)} %constant.60) | copy-start | bytes 28
  8.4 25.9 %copy-start = (bf16[192,2048]{1,0:T(8,128)(2,1)S(1)}, bf16[192,2048]{1,0:T(8,128)(2,1)}, u32[]{:S(2)}) copy-start(bf16[192,2048]{1,0:T(8,128)(2,1)} %param.10) | copy-start | bytes 2359300
  56.5 11.5 %copy-start.7 = (f32[64,128]{1,0:T(8,128)S(1)}, f32[64,128]{1,0:T(8,128)}, u32[]{:S(2)}) copy-start(f32[64,128]{1,0:T(8,128)} %param.15) | copy-start | bytes 98308
  56.5 11.5 %copy-start.8 = (f32[64,128]{1,0:T(8,128)S(1)}, f32[64,128]{1,0:T(8,128)}, u32[]{:S(2)}) copy-start(f32[64,128]{1,0:T(8,128)} %param.16) | copy-start | bytes 98308
  56.5 11.5 %copy-start.11 = (f32[64]{0:T(128)S(1)}, f32[64]{0:T(128)}, u32[]{:S(2)}) copy-start(f32[64]{0:T(128)} %param.11) | copy-start | bytes 772
  56.5 51.6 %all-to-all-start.5 = ((bf16[32,2,6,2048]{3,1,2,0:T(2,128)(2,1)}), bf16[32,2,6,2048]{3,1,2,0:T(2,128)(2,1)S(1)}, u32[]{:S(2)}, u32[]{:S(2)}) async-start(bf16[32,2,6,2048]{3,1,2,0:T(2,128)(2,1)} %copy.64), calls=%async_computation.5 | async-start | bytes 3145728 | tf_op jit(solution)/shard_map/all_to_all | solution.py:117
  67.9 134.4 %all-gather.4.cloned.1.call-start = ((), (), s32[]{:S(2)}) async-start(), calls=%async_computation.7 | async-start | bytes 1081344 | tf_op jit(solution)/shard_map/all_gather | solution.py:46
  68.7 153.4 %all-gather.6.cloned.1.call-start = ((), (), s32[]{:S(2)}) async-start(), calls=%async_computation.8 | async-start | bytes 14155776 | tf_op jit(solution)/shard_map/all_gather | solution.py:118
  138.2 21.3 %all-to-all-start.1 = ((bf16[32,1,2,32,128]{4,3,2,1,0:T(8,128)(2,1)}), bf16[32,1,2,32,128]{4,3,2,1,0:T(8,128)(2,1)S(1)}, u32[]{:S(2)}, u32[]{:S(2)}) async-start(bf16[32,1,2,32,128]{4,3,2,1,0:T(8,128)(2,1)} %get-tuple-element.12), calls=%async_computation.1 | async-start | bytes 1048576 | tf_op jit(solution)/shard_map/all_to_all | solution.py:36
  180.5 21.7 %all-to-all-start.3 = ((bf16[32,1,2,32,128]{4,3,2,1,0:T(8,128)(2,1)}), bf16[32,1,2,32,128]{4,3,2,1,0:T(8,128)(2,1)S(1)}, u32[]{:S(2)}, u32[]{:S(2)}) async-start(bf16[32,1,2,32,128]{4,3,2,1,0:T(8,128)(2,1)} %get-tuple-element.10), calls=%async_computation.3 | async-start | bytes 1048576 | tf_op jit(solution)/shard_map/all_to_all | solution.py:36
  185.1 119.6 %all-gather.8.cloned.1.call-start = ((), (), s32[]{:S(2)}) async-start(), calls=%async_computation.9 | async-start | bytes 7520256 | tf_op jit(solution)/shard_map/all_gather | solution.py:53
  185.6 36.6 %copy-start.3 = (bf16[1,2,32,64,128]{4,3,2,1,0:T(8,128)(2,1)}, bf16[1,2,32,64,128]{4,3,2,1,0:T(8,128)(2,1)S(1)}, u32[]{:S(2)}) copy-start(bf16[1,2,32,64,128]{4,3,2,1,0:T(8,128)(2,1)S(1)} %copy.55) | copy-start | bytes 3145732
  202.3 37.9 %copy-start.4 = (bf16[1,2,32,64,128]{4,3,2,1,0:T(8,128)(2,1)}, bf16[1,2,32,64,128]{4,3,2,1,0:T(8,128)(2,1)S(1)}, u32[]{:S(2)}) copy-start(bf16[1,2,32,64,128]{4,3,2,1,0:T(8,128)(2,1)S(1)} %copy.56) | copy-start | bytes 3145732
  204.1 0.8 copy-start.6
  204.1 36.1 %copy-start.2 = (bf16[2048,128]{1,0:T(8,128)(2,1)}, bf16[2048,128]{1,0:T(8,128)(2,1)S(1)}, u32[]{:S(2)}) copy-start(bf16[2048,128]{1,0:T(8,128)(2,1)S(1)} %get-tuple-element.34) | copy-start | bytes 1572868
  254.0 1.9 copy-start.1
  294.2 10.6 %copy-start.5 = (bf16[1,2,32,32,256]{4,3,2,1,0:T(8,128)(2,1)}, bf16[1,2,32,32,256]{4,3,2,1,0:T(8,128)(2,1)S(1)}, u32[]{:S(2)}) copy-start(bf16[1,2,32,32,256]{4,3,2,1,0:T(8,128)(2,1)S(1)} %copy.57) | copy-start | bytes 3145732
  304.8 2.8 slice-start
  310.8 10.0 %copy-start.10 = (f32[192,8]{0,1:T(8,128)S(1)}, f32[192,8]{0,1:T(8,128)}, u32[]{:S(2)}) copy-start(f32[192,8]{0,1:T(8,128)} %param.19) | copy-start | bytes 18436
  310.8 10.1 %copy-start.9 = (f32[32,256]{1,0:T(8,128)S(1)}, f32[32,256]{1,0:T(8,128)}, u32[]{:S(2)}) copy-start(f32[32,256]{1,0:T(8,128)} %param.17) | copy-start | bytes 98308
  310.8 88.9 %all-to-all-start.6 = ((bf16[32,2,48,256]{3,2,1,0:T(8,128)(2,1)}), bf16[32,2,48,256]{3,2,1,0:T(8,128)(2,1)S(1)}, u32[]{:S(2)}, u32[]{:S(2)}) async-start(bf16[32,2,48,256]{3,2,1,0:T(8,128)(2,1)} %copy.70), calls=%async_computation.6 | async-start | bytes 3145728 | tf_op jit(solution)/shard_map/all_to_all | solution.py:132
Sparse Core Ops, SparseCore 0:
  71.9 81.0 all-gather.3
  154.8 67.2 all-gather.5
  255.2 49.5 all-gather.7
where the time goes:
time: 416 us; the launch traced here: 414 us
  blocking collectives  162 us (39%)
  waiting for transfers between devices  99.9 us (24%)
  local copies, waits for them, and re-layouts  46.9 us (11%)
  matrix products  36.3 us (9%)
  starting transfers between devices  30.3 us (7%)
  other arithmetic  24.6 us (6%)
  between operations  14.2 us (3%)
    all_gather x1, blocking collectives, body(): lax.all_gather(shared_third_local, 'fs', axis=0, tiled=True)  78.8 us
    all_to_all x2, blocking collectives, several_exchanges(): lax.all_to_all(share, axis, split_axis=0, concat_axis=0, tiled=True)  45.2 us
    all_to_all x1, waiting for transfers between devices, body(): lax.all_to_all(mine, 'fs', split_axis=0, concat_axis=0, tiled=True)  39.3 us
    all_to_all x1, blocking collectives, body(): lax.all_to_all(down_local, 'fs', split_axis=0, concat_axis=2, tiled=True)  38.1 us
    all_to_all x2, waiting for transfers between devices, several_exchanges(): lax.all_to_all(share, axis, split_axis=0, concat_axis=0, tiled=True)  33 us
    another operation x3, other arithmetic  18.4 us
    dot_general x1, matrix products, expert_hidden(): jnp.einsum('secn,enf->secf', rows, gate_new, preferred_element_type=jnp.f...  18 us
    all_gather x1, waiting for transfers between devices, body(): lax.all_gather(arrived, 'tp', axis=2, tiled=True)  16.9 us
  transfers between devices with their start and end apart: 7, of which 5 were waited for; matrix products, arithmetic and copies ran while one was open for 3% of the time, Pallas kernels for 0%

commit v1 on v0

v1 whole, which is shorter than its diff:
```python
import jax
import jax.numpy as jnp
from jax import lax
from jax.experimental import pallas as pl
from jax.experimental.pallas import tpu as pltpu
from jax.sharding import PartitionSpec as P

EPS = 1e-06
NZ, NX, NY = 8, 4, 4
NF, NT = NZ * NX, NY * 2
D, DE, TOK, TOP_K, EXPERTS = 2048, 1024, 192, 8, 64
CAP = 2 * TOK * TOP_K // EXPERTS
PER = EXPERTS // NF
DC = D // NT
HC = DE // NT
KR, KD = D // NF, DE // NF
ROWS = TOK + KR + KD + 16
CUT = 160
SRC = NX * CAP
OFFS = (0, -1, 1, -2, 2, -3, 3, 4)
BF, F32 = jnp.bfloat16, jnp.float32
MESH = pl.DeviceIdType.MESH


def silu_mul(a, b):
    return (a * (1.0 / (1.0 + jnp.exp(-a)))) * b


def kernel(
    tblk, nfull, wgu, wdn,
    gu_o, dn_o, sw_o, ret_o, sh_o,
    ta, xg, gu, dn, hg, hs, og, ret, shv,
    zr, xr, br, bs, cr, cs, er, dr, ss, lo,
):
    fs, tp = lax.axis_index("fs"), lax.axis_index("tp")
    z, x = fs // NX, lax.rem(fs, NX)
    y, c = tp // 2, lax.rem(tp, 2)

    def fsn(dz, dx):
        return lax.rem(z + dz + NZ, NZ) * NX + lax.rem(x + dx + NX, NX)

    def tpn(dy, dc):
        return lax.rem(y + dy + NY, NY) * 2 + lax.rem(c + dc, 2)

    yp, ym, sib = tpn(1, 0), tpn(-1, 0), tpn(0, 1)

    def copy(src, dst, s, r, f, t):
        return pltpu.make_async_remote_copy(
            src_ref=src, dst_ref=dst, send_sem=s, recv_sem=r, device_id=(f, t), device_id_type=MESH
        )

    def arrived(dst, r):
        copy(dst, dst, ss.at[0], r, fs, sib).wait_recv()

    barrier = pltpu.get_barrier_semaphore()
    for k in range(1, NF):
        pl.semaphore_signal(barrier, inc=1, device_id=(lax.rem(fs + k, NF), tp), device_id_type=MESH)
    for t in (yp, ym, sib):
        pl.semaphore_signal(barrier, inc=1, device_id=(fs, t), device_id_type=MESH)
    pl.semaphore_wait(barrier, NF - 1 + 3)

    zp, zm, xp, xm = fsn(1, 0), fsn(-1, 0), fsn(0, 1), fsn(0, -1)

    def zi(i):
        return lax.rem(z + OFFS[i] + NZ, NZ)

    def z_step(i):
        s = zi(i) * NX + x
        blk = ta.at[s]
        if i == 0:
            copy(tblk, blk, ss.at[0], zr.at[1], zp, tp).start()
            copy(tblk, blk, ss.at[0], zr.at[2], zm, tp).start()
            copy(tblk, blk, ss.at[0], xr.at[0, 0], xp, tp).start()
            copy(tblk, blk, ss.at[0], xr.at[0, 1], xm, tp).start()
            ta[fs] = tblk[...]
            return
        low, high = ta.at[s, pl.ds(0, CUT)], ta.at[s, pl.ds(CUT, ROWS - CUT)]
        if i == 7:
            arrived(low, zr.at[7])
            arrived(high, zr.at[8])
        else:
            arrived(blk, zr.at[i])
            if i == 5:
                copy(low, low, ss.at[0], zr.at[7], zp, tp).start()
            elif i == 6:
                copy(high, high, ss.at[0], zr.at[8], zm, tp).start()
            else:
                copy(blk, blk, ss.at[0], zr.at[i + 2], zp if OFFS[i] < 0 else zm, tp).start()
        copy(blk, blk, ss.at[0], xr.at[i, 0], xp, tp).start()
        copy(blk, blk, ss.at[0], xr.at[i, 1], xm, tp).start()

    def x_step(i):
        left = zi(i) * NX + lax.rem(x + NX - 1, NX)
        right = zi(i) * NX + lax.rem(x + 1, NX)
        arrived(ta.at[left], xr.at[i, 0])
        low = ta.at[left, pl.ds(0, CUT)]
        copy(low, low, ss.at[0], xr.at[i, 2], xp, tp).start()
        arrived(ta.at[right], xr.at[i, 1])
        high = ta.at[right, pl.ds(CUT, ROWS - CUT)]
        copy(high, high, ss.at[0], xr.at[i, 3], xm, tp).start()

    cols = pl.ds(pl.multiple_of(tp * DC, DC), DC)
    hcols = pl.ds(pl.multiple_of(tp * HC, HC), HC)

    def select(i):
        far = zi(i) * NX + lax.rem(x + 2, NX)
        arrived(ta.at[far, pl.ds(0, CUT)], xr.at[i, 2])
        arrived(ta.at[far, pl.ds(CUT, ROWS - CUT)], xr.at[i, 3])
        first = (PER * fs).astype(F32)
        rows = []
        for k in range(NX):
            ids = ta[zi(i) * NX + k, pl.ds(ROWS - 16, 16), pl.ds(0, TOK)].astype(F32)
            for e in range(PER):
                rows.append(jnp.sum(jnp.where(ids == first + e, 1.0, 0.0), axis=0, keepdims=True))
        match = jnp.concatenate(rows, axis=0)
        before = (
            lax.broadcasted_iota(jnp.int32, (TOK, TOK), 0) < lax.broadcasted_iota(jnp.int32, (TOK, TOK), 1)
        )
        upper = jnp.where(before, 1.0, 0.0).astype(BF)
        rank = jnp.dot(match.astype(BF), upper, preferred_element_type=F32)
        place = jnp.where(match > 0.5, rank, -1.0)
        slot = lax.broadcasted_iota(jnp.int32, (CAP, TOK), 0).astype(F32)
        for k in range(NX):
            hot = jnp.concatenate(
                [jnp.where(slot == place[PER * k + e : PER * k + e + 1], 1.0, 0.0) for e in range(PER)], axis=0
            ).astype(BF)
            rows = jnp.dot(hot, ta[zi(i) * NX + k, pl.ds(0, TOK), :], preferred_element_type=F32).astype(BF)
            for e in range(PER):
                xg[i, e, pl.ds(CAP * k, CAP), cols] = rows[CAP * e : CAP * (e + 1)]

    def at(buf, i, w, t):
        return buf.at[i, :, :, pl.ds(pl.multiple_of(t * w, w), w)]

    def half(buf, i, w, t, e):
        return buf.at[i, e, :, pl.ds(pl.multiple_of(t * w, w), w)]

    def tp_send(buf, i, w, s, r, b):
        own = at(buf, i, w, tp)
        copy(own, own, s, r.at[0], fs, yp).start()
        copy(own, own, s, r.at[1], fs, ym).start()
        copy(own, own, s, b, fs, sib).start()

    def tp_pass(buf, i, w, s, r, b):
        a = at(buf, i, w, ym)
        arrived(a, r.at[0])
        h = half(buf, i, w, ym, 0)
        copy(h, h, s, r.at[2], fs, yp).start()
        copy(a, a, s, b, fs, sib).start()
        a = at(buf, i, w, yp)
        arrived(a, r.at[1])
        h = half(buf, i, w, yp, 1)
        copy(h, h, s, r.at[3], fs, ym).start()
        copy(a, a, s, b, fs, sib).start()

    def tp_last(buf, i, w, s, r, b):
        far = tpn(2, 0)
        for e in range(2):
            h = half(buf, i, w, far, e)
            arrived(h, r.at[2 + e])
            copy(h, h, s, b, fs, sib).start()

    def tp_done(buf, i, w, b):
        arrived(buf.at[i, :, :, pl.ds(0, 4 * w)], b)

    peers = [(dz, dx) for dx in (0, 1, 3, 2) for dz in (1, -1, 2, -2, 3, -3, 4, 0)]
    peers = [p for p in peers if p != (0, 0)]

    def send_gu(n):
        f = fsn(*peers[n])
        copy(wgu.at[f], gu.at[:, pl.ds(pl.multiple_of(fs * KR, KR), KR), :], ss.at[3], er.at[0], f, tp).start()

    def send_dn(n):
        f = fsn(*peers[n])
        copy(wdn.at[f], dn.at[:, pl.ds(pl.multiple_of(fs * KD, KD), KD), :], ss.at[4], er.at[1], f, tp).start()

    def gate_up(i):
        for e in range(PER):
            both = jnp.dot(xg[i, e], gu[e], preferred_element_type=F32)
            hg[i, e, :, hcols] = silu_mul(both[:, :HC], both[:, HC:]).astype(BF)

    def down(i):
        for e in range(PER):
            out = jnp.dot(hg[i, e], dn[e], preferred_element_type=F32).astype(BF)
            for k in range(NX):
                og[i, k, pl.ds(CAP * e, CAP), :] = out[CAP * k : CAP * (k + 1)]

    def give_back(i):
        for dx in range(NX):
            k = lax.rem(x + dx, NX)
            if i == 0 and dx == 0:
                ret[fs] = og[0, k]
                continue
            copy(og.at[i, k], ret.at[fs], ss.at[5], dr.at[0], zi(i) * NX + k, tp).start()

    sent_gu, sent_dn = 0, 0
    for tick in range(NZ + 4):
        if tick < NZ:
            z_step(tick)
        if 0 <= tick - 1 < NZ:
            x_step(tick - 1)
        if 0 <= tick - 2 < NZ:
            select(tick - 2)
            tp_send(xg, tick - 2, DC, ss.at[1], br.at[tick - 2], bs.at[tick - 2])
        if 0 <= tick - 3 < NZ:
            tp_pass(xg, tick - 3, DC, ss.at[1], br.at[tick - 3], bs.at[tick - 3])
        if 0 <= tick - 4 < NZ:
            tp_last(xg, tick - 4, DC, ss.at[1], br.at[tick - 4], bs.at[tick - 4])
        for _ in range(4):
            if sent_gu < NF - 1:
                send_gu(sent_gu)
                sent_gu += 1
        if tick == 0:
            gu[:, pl.ds(pl.multiple_of(fs * KR, KR), KR), :] = wgu[fs]
            dn[:, pl.ds(pl.multiple_of(fs * KD, KD), KD), :] = wdn[fs]
        if tick >= NZ:
            for _ in range(8):
                if sent_dn < NF - 1:
                    send_dn(sent_dn)
                    sent_dn += 1
        if tick == NZ + 2:
            sgu = ta[:, pl.ds(TOK, KR), :].reshape(D, 2 * HC)
            both = jnp.dot(nfull[...], sgu, preferred_element_type=F32)
            mid = silu_mul(both[:, :HC], both[:, HC:]).astype(BF)
            hs[0, 0, :, hcols] = mid[: TOK // 2]
            hs[0, 1, :, hcols] = mid[TOK // 2 :]

    shared = (hs, 0, HC, ss.at[6], cr.at[NZ], cs.at[NZ])
    tp_send(*shared)
    arrived(gu.at[:, pl.ds(0, D - KR), :], er.at[0])
    gu_copy = pltpu.make_async_copy(gu, gu_o, lo.at[0])
    gu_copy.start()
    for tick in range(NZ + 3):
        if tick < NZ:
            tp_done(xg, tick, DC, bs.at[tick])
            gate_up(tick)
            tp_send(hg, tick, HC, ss.at[2], cr.at[tick], cs.at[tick])
        if tick == 0:
            tp_pass(*shared)
        elif tick == 1:
            tp_last(*shared)
        if 0 <= tick - 1 < NZ:
            tp_pass(hg, tick - 1, HC, ss.at[2], cr.at[tick - 1], cs.at[tick - 1])
        if 0 <= tick - 2 < NZ:
            tp_last(hg, tick - 2, HC, ss.at[2], cr.at[tick - 2], cs.at[tick - 2])
        if 0 <= tick - 3 < NZ:
            if tick == 3:
                arrived(dn.at[:, pl.ds(0, DE - KD), :], er.at[1])
                dn_copy = pltpu.make_async_copy(dn, dn_o, lo.at[1])
                dn_copy.start()
            tp_done(hg, tick - 3, HC, cs.at[tick - 3])
            down(tick - 3)
            give_back(tick - 3)
    sw_copy = pltpu.make_async_copy(ta.at[:, pl.ds(TOK, KR + KD), :], sw_o, lo.at[2])
    sw_copy.start()
    tp_done(hs, 0, HC, cs.at[NZ])
    sdn = ta[:, pl.ds(TOK + KR, KD), :].reshape(DE, DC)
    for e in range(2):
        shv[pl.ds(e * (TOK // 2), TOK // 2), :] = jnp.dot(hs[0, e], sdn, preferred_element_type=F32)
    sh_copy = pltpu.make_async_copy(shv, sh_o, lo.at[3])
    sh_copy.start()
    arrived(ret.at[pl.ds(0, NF - 1)], dr.at[0])
    ret_copy = pltpu.make_async_copy(ret, ret_o, lo.at[4])
    ret_copy.start()

    def sent(ref, s):
        copy(ref, ref, s, dr.at[0], fs, sib).wait_send()

    sent(ta.at[pl.ds(0, NF - 1)], ss.at[0])
    sent(xg.at[pl.ds(0, NZ - 1)], ss.at[1])
    sent(hg.at[pl.ds(0, NZ - 1)], ss.at[2])
    sent(gu.at[:, pl.ds(0, D - KR), :], ss.at[3])
    sent(dn.at[:, pl.ds(0, DE - KD), :], ss.at[4])
    sent(ret.at[pl.ds(0, NF - 1)], ss.at[5])
    sent(hs.at[0, :, :, pl.ds(0, 7 * HC)], ss.at[6])
    gu_copy.wait()
    dn_copy.wait()
    sw_copy.wait()
    sh_copy.wait()
    ret_copy.wait()


def exchange(tblk, nfull, wgu, wdn):
    vmem, anyw = pl.BlockSpec(memory_space=pltpu.VMEM), pl.BlockSpec(memory_space=pl.ANY)
    dma = pltpu.SemaphoreType.DMA
    return pl.pallas_call(
        kernel,
        out_shape=(
            jax.ShapeDtypeStruct((PER, D, 2 * HC), BF),
            jax.ShapeDtypeStruct((PER, DE, DC), BF),
            jax.ShapeDtypeStruct((NF, KR + KD, DC), BF),
            jax.ShapeDtypeStruct((NF, PER * CAP, DC), BF),
            jax.ShapeDtypeStruct((TOK, DC), F32),
        ),
        in_specs=[vmem] * 4,
        out_specs=(anyw,) * 5,
        scratch_shapes=[
            pltpu.VMEM((NF, ROWS, DC), BF),
            pltpu.VMEM((NZ, PER, SRC, D), BF),
            pltpu.VMEM((PER, D, 2 * HC), BF),
            pltpu.VMEM((PER, DE, DC), BF),
            pltpu.VMEM((NZ, PER, SRC, DE), BF),
            pltpu.VMEM((1, 2, TOK // 2, DE), BF),
            pltpu.VMEM((NZ, NX, PER * CAP, DC), BF),
            pltpu.VMEM((NF, PER * CAP, DC), BF),
            pltpu.VMEM((TOK, DC), F32),
            dma((9,)), dma((NZ, 4)), dma((NZ, 4)), dma((NZ,)), dma((NZ + 1, 4)), dma((NZ + 1,)),
            dma((2,)), dma((1,)), dma((7,)), dma((5,)),
        ],
        compiler_params=pltpu.CompilerParams(
            collective_id=0, has_side_effects=True, vmem_limit_bytes=56 * 1024 * 1024
        ),
    )(tblk, nfull, wgu, wdn)


def body(
    tokens,
    norm_gain,
    expert_gate,
    expert_up,
    expert_down,
    shared_gate,
    shared_up,
    shared_down,
    expert_ids,
    route_weights,
):
    gain = norm_gain[None, :, None]
    wgu = jnp.concatenate([expert_gate * gain, expert_up * gain], axis=2).astype(BF).reshape(NF, PER, KR, 2 * HC)
    wdn = expert_down.astype(BF).reshape(NF, PER, KD, DC)
    sgu = (jnp.concatenate([shared_gate, shared_up], axis=1) * norm_gain[:, None]).astype(BF)
    wide = tokens.astype(F32)
    normed = (wide * lax.rsqrt(jnp.mean(wide * wide, axis=-1, keepdims=True) + EPS)).astype(BF)
    mine = lax.dynamic_slice_in_dim(normed, lax.axis_index("tp") * DC, DC, 1)
    ids = jnp.pad(expert_ids.T, ((0, 16 - TOP_K), (0, DC - TOK)), constant_values=EXPERTS).astype(BF)
    tblk = jnp.concatenate([mine, sgu, shared_down.astype(BF), ids], axis=0)
    gu, dn, sw, ret, shared = exchange(tblk, normed, wgu, wdn)
    hit = expert_ids[:, :, None] == jnp.arange(EXPERTS, dtype=jnp.int32)
    match = jnp.sum(hit.astype(F32), axis=1)
    weight = jnp.sum(jnp.where(hit, route_weights[:, :, None], 0.0), axis=1)
    low = jnp.tril(jnp.ones((TOK, TOK), BF), -1)
    rank = jnp.dot(low, match.astype(BF), preferred_element_type=F32).astype(jnp.int32)
    mix = jnp.where(
        rank[:, :, None] == jnp.arange(CAP, dtype=jnp.int32), weight[:, :, None], 0.0
    ).reshape(TOK, EXPERTS * CAP)
    high = mix.astype(BF)
    rest = (mix - high.astype(F32)).astype(BF)
    rows = ret.reshape(EXPERTS * CAP, DC)
    routed = jnp.dot(high, rows, preferred_element_type=F32) + jnp.dot(rest, rows, preferred_element_type=F32)
    return (
        gu[:, :, :HC],
        gu[:, :, HC:],
        dn,
        sw[:, :KR, :HC].reshape(D, HC),
        sw[:, :KR, HC:].reshape(D, HC),
        sw[:, KR:, :].reshape(DE, DC),
        (shared + routed).astype(BF),
    )


def solution(mesh):
    in_specs = (
        P("fs", None),
        P("fs"),
        P(None, "fs", "tp"),
        P(None, "fs", "tp"),
        P(None, "fs", "tp"),
        P("fs", "tp"),
        P("fs", "tp"),
        P("fs", "tp"),
        P("fs", None),
        P("fs", None),
    )
    out_specs = (
        P("fs", None, "tp"),
        P("fs", None, "tp"),
        P("fs", None, "tp"),
        P(None, "tp"),
        P(None, "tp"),
        P(None, "tp"),
        P("fs", "tp"),
    )
    return jax.shard_map(body, mesh=mesh, in_specs=in_specs, out_specs=out_specs, check_vma=False)
```

time: 416 us -> 182 us (0.44)
  blocking collectives: 162 us -> 0 us
  Pallas kernels: 0 us -> 161 us
  waiting for transfers between devices: 99.9 us -> 0 us
  local copies, waits for them, and re-layouts: 46.9 us -> 5.32 us
  matrix products: 36.3 us -> 3.7 us
  starting transfers between devices: 30.3 us -> 0 us
  other arithmetic: 24.6 us -> 10.5 us
  between operations: 14.2 us -> 0.88 us
    pallas_call x0 -> x1, Pallas kernels: none -> 161 us  [exchange(): pl.pallas_call(kernel, out_shape=(jax.ShapeDtypeStruct((PER, D, 2 * HC),...]
    all_to_all x3 -> x0, blocking collectives: 83.3 us -> none  [the longest x2 45.2 us: several_exchanges(): lax.all_to_all(share, axis, split_axis=0, concat_axis=0, tiled=True)]
    all_gather x1 -> x0, blocking collectives: 78.8 us -> none  [body(): lax.all_gather(shared_third_local, 'fs', axis=0, tiled=True)]
    all_to_all x4 -> x0, waiting for transfers between devices: 72.4 us -> none  [the longest x1 39.3 us: body(): lax.all_to_all(mine, 'fs', split_axis=0, concat_axis=0, tiled=True)]
    dot_general x6 -> x3, matrix products: 36.3 us -> 3.7 us  [the longest x1 2.14 us: body(): jnp.dot(high, rows, preferred_element_type=F32)]
    all_to_all x4 -> x0, starting transfers between devices: 29.9 us -> none  [the longest x1 11.4 us: body(): lax.all_to_all(mine, 'fs', split_axis=0, concat_axis=0, tiled=True)]
    all_gather x3 -> x0, waiting for transfers between devices: 27.5 us -> none  [the longest x1 16.9 us: body(): lax.all_gather(arrived, 'tp', axis=2, tiled=True)]
    gather x2 -> x0, local copies, waits for them, and re-layouts: 20.7 us -> none  [the longest x1 15.9 us: body(): normed[slot_token.reshape(-1)]]
  transfers between devices with their start and end apart: 7 -> 0, of which waited for: 5 -> 0; matrix products, arithmetic and copies ran while one was open for 3% -> 0% of each run, Pallas kernels for 0% -> 0%
where the time goes in v1:
time: 182 us
  Pallas kernels  161 us (88%)
  other arithmetic  10.5 us (6%)
  local copies, waits for them, and re-layouts  5.32 us (3%)
  matrix products  3.7 us (2%)
    pallas_call x1, Pallas kernels, exchange(): pl.pallas_call(kernel, out_shape=(jax.ShapeDtypeStruct((PER, D, 2 * HC),...  161 us

profile of v1, /device:TPU:8, one launch (start us, length us, event | category | flops | bytes accessed | tf_op | source)
XLA Modules:
  0.0 181.5 jit_solution(11326629990895203717)
XLA Ops:
  0.6 0.0 copy-start.11
  0.6 0.0 copy-start.8
  0.7 0.0 copy-start.7
  0.7 0.0 copy-start.9
  0.7 0.0 copy-start.6
  0.7 0.0 copy-start.1
  0.7 1.5 fusion.1
  2.2 1.3 fusion.2.nfull
  3.6 0.0 copy-start
  3.6 0.0 copy-done.11
  3.6 0.0 copy-done.8
  3.6 0.0 copy-done.7
  3.6 0.1 fusion.10
  3.7 0.0 copy-done.9
  3.7 0.0 copy-done.6
  3.8 0.7 fusion.7.tblk
  4.5 0.0 copy-done.1
  4.5 2.2 %multiply_convert_fusion.1 = (bf16[64,64,128]{2,1,0:T(8,128)(2,1)S(1)}, bf16[64,64,128]{2,1,0:T(8,128)(2,1)S(1)}) fusion(f32[64,64,128]{2,1,0:T(8,128)S(1)} %copy-done.1, f32[64]{0:T(128)S(1)} %copy-done.11, f32[64,64,128]{2,1,0:T(8,128)} %param.13), kind=kLoop, calls=%fused_computation.6 | loop fusion | flops 2097152 | bytes 6291712 | tf_op jit(solution)/shard_map/convert.3
  6.7 0.0 copy-done
  6.7 0.0 copy-start.2
  6.7 1.7 pad_maximum_fusion.wgu
  8.4 0.5 copy-done.2
  8.9 1.1 convert_element_type.75
  10.0 0.0 copy-start.10
  10.0 161.2 %shard_map.153 = (bf16[2,2048,256]{2,1,0:T(8,128)(2,1)}, bf16[2,1024,256]{2,1,0:T(8,128)(2,1)}, bf16[32,96,256]{2,1,0:T(8,128)(2,1)}, bf16[32,96,256]{2,1,0:T(8,128)(2,1)}, f32[192,256]{1,0:T(8,128)}) custom-call(bf16[304,256]{1,0:T(8,128)(2,1)} %fusion.7.tblk, bf16[192,2048]{1,0:T(8,128)(2,1)} %copy-done, bf16[32,2,64,256]{3,2,1,0:T(8,128)(2,1)} %pad_maximum_fusion.wgu, ...), custom_call_target="tpu_custom_call" | custom-call | tf_op jit(solution)/shard_map/pallas_call | solution.py:285
  171.2 0.0 copy-done.10
  171.2 0.1 convert_reduce_fusion
  171.3 0.2 convolution_convert_fusion
  171.5 0.9 select_convert_fusion
  172.5 0.0 copy-start.12
  172.5 0.0 copy-start.13
  172.5 2.1 %fusion.18 = f32[192,256]{1,0:T(8,128)S(1)} fusion(bf16[192,3072]{0,1:T(8,128)(2,1)S(1)} %bitcast.20, bf16[3072,256]{1,0:T(8,128)(2,1)} %bitcast.24), kind=kOutput, calls=%fused_computation.37 | convolution fusion | flops 301989888 | bytes 2949120 | tf_op jit(solution)/shard_map/dot_general | solution.py:348
  174.7 0.7 fusion
  175.4 0.0 copy-start.4
  175.4 0.0 copy-done.12
  175.4 0.0 copy-done.13
  175.4 0.0 copy-start.3
  175.4 1.3 fusion.4
  176.7 0.0 copy-done.4
  176.8 1.3 fusion.17
  178.0 0.0 copy-done.3
  178.0 0.0 copy-start.5
  178.1 1.7 fusion.16
  179.7 0.8 slice.19
  180.6 0.0 copy-done.5
  180.6 1.0 copy.23
  (5 shorter events, 0.0 us)
Async XLA Ops:
  0.6 3.0 %copy-start.11 = (f32[64]{0:T(128)S(1)}, f32[64]{0:T(128)}, u32[]{:S(2)}) copy-start(f32[64]{0:T(128)} %param.11) | copy-start | bytes 772
  0.6 3.0 %copy-start.8 = (f32[64,128]{1,0:T(8,128)S(1)}, f32[64,128]{1,0:T(8,128)}, u32[]{:S(2)}) copy-start(f32[64,128]{1,0:T(8,128)} %param.15) | copy-start | bytes 98308
  0.7 3.0 %copy-start.7 = (f32[64,128]{1,0:T(8,128)S(1)}, f32[64,128]{1,0:T(8,128)}, u32[]{:S(2)}) copy-start(f32[64,128]{1,0:T(8,128)} %param.16) | copy-start | bytes 98308
  0.7 3.1 %copy-start.9 = (f32[32,256]{1,0:T(8,128)S(1)}, f32[32,256]{1,0:T(8,128)}, u32[]{:S(2)}) copy-start(f32[32,256]{1,0:T(8,128)} %param.17) | copy-start | bytes 98308
  0.7 3.1 %copy-start.6 = (s32[192,8]{0,1:T(8,128)S(1)}, s32[192,8]{0,1:T(8,128)}, u32[]{:S(2)}) copy-start(s32[192,8]{0,1:T(8,128)} %param.18) | copy-start | bytes 18436
  0.7 3.8 %copy-start.1 = (f32[64,64,128]{2,1,0:T(8,128)S(1)}, f32[64,64,128]{2,1,0:T(8,128)}, u32[]{:S(2)}) copy-start(f32[64,64,128]{2,1,0:T(8,128)} %param.12) | copy-start | bytes 6291460
  3.6 3.1 %copy-start = (bf16[192,2048]{1,0:T(8,128)(2,1)}, bf16[192,2048]{1,0:T(8,128)(2,1)S(1)}, u32[]{:S(2)}) copy-start(bf16[192,2048]{1,0:T(8,128)(2,1)S(1)} %fusion.2.nfull) | copy-start | bytes 2359300
  6.7 2.2 %copy-start.2 = (f32[64,32,256]{2,1,0:T(8,128)S(1)}, f32[64,32,256]{2,1,0:T(8,128)}, u32[]{:S(2)}) copy-start(f32[64,32,256]{2,1,0:T(8,128)} %param.14) | copy-start | bytes 6291460
  10.0 161.2 %copy-start.10 = (f32[192,8]{0,1:T(8,128)S(1)}, f32[192,8]{0,1:T(8,128)}, u32[]{:S(2)}) copy-start(f32[192,8]{0,1:T(8,128)} %param.19) | copy-start | bytes 18436
  172.5 2.9 %copy-start.12 = (bf16[32,96,256]{2,1,0:T(8,128)(2,1)S(1)}, bf16[32,96,256]{2,1,0:T(8,128)(2,1)}, u32[]{:S(2)}) copy-start(bf16[32,96,256]{2,1,0:T(8,128)(2,1)} %get-tuple-element.16) | copy-start | bytes 4718596
  172.5 2.9 %copy-start.13 = (f32[192,256]{1,0:T(8,128)S(1)}, f32[192,256]{1,0:T(8,128)}, u32[]{:S(2)}) copy-start(f32[192,256]{1,0:T(8,128)} %get-tuple-element.15) | copy-start | bytes 589828
  175.4 1.4 copy-start.4
  175.4 2.7 %copy-start.3 = (bf16[2,2048,256]{2,1,0:T(8,128)(2,1)S(1)}, bf16[2,2048,256]{2,1,0:T(8,128)(2,1)}, u32[]{:S(2)}) copy-start(bf16[2,2048,256]{2,1,0:T(8,128)(2,1)} %get-tuple-element.12) | copy-start | bytes 6291460
  178.0 2.5 %copy-start.5 = (bf16[2,1024,256]{2,1,0:T(8,128)(2,1)S(1)}, bf16[2,1024,256]{2,1,0:T(8,128)(2,1)}, u32[]{:S(2)}) copy-start(bf16[2,1024,256]{2,1,0:T(8,128)(2,1)} %get-tuple-element.34) | copy-start | bytes 3145732

commit v2 on v1

v2 whole, which is shorter than its diff:
```python
import jax
import jax.numpy as jnp
from jax import lax
from jax.experimental import pallas as pl
from jax.experimental.pallas import tpu as pltpu
from jax.sharding import PartitionSpec as P

EPS = 1e-06
NZ, NX, NY = 8, 4, 4
NF, NT = NZ * NX, NY * 2
D, DE, TOK, TOP_K, EXPERTS = 2048, 1024, 192, 8, 64
CAP = 2 * TOK * TOP_K // EXPERTS
PER = EXPERTS // NF
DC = D // NT
HC = DE // NT
KR, KD = D // NF, DE // NF
SRC = NX * CAP
ROW_EXPERTS = NX * PER
OFFS = (0, -1, 1, -2, 2, -3, 3, 4)
ORDER = (4, 3, 6, 5, 7, 2, 1, 0)
BF, F32 = jnp.bfloat16, jnp.float32
MESH = pl.DeviceIdType.MESH


def silu_mul(a, b):
    return (a * (1.0 / (1.0 + jnp.exp(-a)))) * b


def kernel(
    tokens, ids_in, rw_in, gain_in, sgate, sup, sdown, gate, up, down_w,
    gate_o, up_o, dn_o, sg_o, su_o, sd_o, mixed_o,
    fg, fu, fd, wgu, wdn, nfull, ta, tb, xg, gu, dn, hg, hs, og, wt, r1, pt, pr, mv,
    zr, xr, szr, sxr, br, bs, cr, cs, er, d1, dr, ss, lo, li,
):
    fs, tp = lax.axis_index("fs"), lax.axis_index("tp")
    z, x = fs // NX, lax.rem(fs, NX)
    y, c = tp // 2, lax.rem(tp, 2)

    def fsn(dz, dx):
        return lax.rem(z + dz + NZ, NZ) * NX + lax.rem(x + dx + NX, NX)

    def tpn(dy, dc):
        return lax.rem(y + dy + NY, NY) * 2 + lax.rem(c + dc, 2)

    yp, ym, sib = tpn(1, 0), tpn(-1, 0), tpn(0, 1)
    cols = pl.ds(pl.multiple_of(tp * DC, DC), DC)
    hcols = pl.ds(pl.multiple_of(tp * HC, HC), HC)

    def copy(src, dst, s, r, f, t):
        return pltpu.make_async_remote_copy(
            src_ref=src, dst_ref=dst, send_sem=s, recv_sem=r, device_id=(f, t), device_id_type=MESH
        )

    def arrived(dst, r):
        copy(dst, dst, ss.at[0], r, fs, sib).wait_recv()

    loads = [pltpu.make_async_copy(a, b, li.at[k]) for k, (a, b) in enumerate(((gate, fg), (up, fu), (down_w, fd)))]
    for load in loads:
        load.start()

    barrier = pltpu.get_barrier_semaphore()
    for k in range(1, NF):
        pl.semaphore_signal(barrier, inc=1, device_id=(lax.rem(fs + k, NF), tp), device_id_type=MESH)
    for t in (yp, ym, sib):
        pl.semaphore_signal(barrier, inc=1, device_id=(fs, t), device_id_type=MESH)

    wide = tokens[...].astype(F32)
    scale = lax.rsqrt(jnp.mean(wide * wide, axis=-1, keepdims=True) + EPS)
    nfull[...] = (wide * scale).astype(BF)
    ta[fs, pl.ds(0, TOK), :] = nfull[:, cols]
    ta[fs, pl.ds(TOK, 16), :] = jnp.zeros((16, DC), BF)
    ta[fs, pl.ds(TOK, 16), pl.ds(0, TOK)] = jnp.concatenate(
        [ids_in[...].astype(F32), rw_in[...]], axis=0
    ).astype(BF)
    diag = lax.broadcasted_iota(jnp.int32, (KR, KR), 0) == lax.broadcasted_iota(jnp.int32, (KR, KR), 1)
    gain = jnp.sum(jnp.where(diag, gain_in[...], 0.0), axis=1, keepdims=True)
    tb[fs, pl.ds(0, KR), pl.ds(0, HC)] = (sgate[...] * gain).astype(BF)
    tb[fs, pl.ds(0, KR), pl.ds(HC, HC)] = (sup[...] * gain).astype(BF)
    tb[fs, pl.ds(KR, KD), :] = sdown[...].astype(BF)
    pl.semaphore_wait(barrier, NF - 1 + 3)

    zp, zm, xp, xm = fsn(1, 0), fsn(-1, 0), fsn(0, 1), fsn(0, -1)

    def zi(i):
        return lax.rem(z + OFFS[i] + NZ, NZ)

    def z_step(buf, i, s, zq, xq):
        at_home = zi(i) * NX + x
        rows = buf.shape[1]
        cut = rows // 32 * 16
        blk = buf.at[at_home]
        low, high = buf.at[at_home, pl.ds(0, cut)], buf.at[at_home, pl.ds(cut, rows - cut)]
        if i == 0:
            copy(blk, blk, s, zq.at[1], zp, tp).start()
            copy(blk, blk, s, zq.at[2], zm, tp).start()
        elif i == 7:
            arrived(low, zq.at[7])
            arrived(high, zq.at[8])
        else:
            arrived(blk, zq.at[i])
            if i == 5:
                copy(low, low, s, zq.at[7], zp, tp).start()
            elif i == 6:
                copy(high, high, s, zq.at[8], zm, tp).start()
            else:
                copy(blk, blk, s, zq.at[i + 2], zp if OFFS[i] < 0 else zm, tp).start()
        copy(blk, blk, s, xq.at[i, 0], xp, tp).start()
        copy(blk, blk, s, xq.at[i, 1], xm, tp).start()

    def x_step(buf, i, s, zq, xq):
        rows = buf.shape[1]
        cut = rows // 32 * 16
        left = zi(i) * NX + lax.rem(x + NX - 1, NX)
        right = zi(i) * NX + lax.rem(x + 1, NX)
        arrived(buf.at[left], xq.at[i, 0])
        low = buf.at[left, pl.ds(0, cut)]
        copy(low, low, s, xq.at[i, 2], xp, tp).start()
        arrived(buf.at[right], xq.at[i, 1])
        high = buf.at[right, pl.ds(cut, rows - cut)]
        copy(high, high, s, xq.at[i, 3], xm, tp).start()

    def x_last(buf, i, s, zq, xq):
        rows = buf.shape[1]
        cut = rows // 32 * 16
        far = zi(i) * NX + lax.rem(x + 2, NX)
        arrived(buf.at[far, pl.ds(0, cut)], xq.at[i, 2])
        arrived(buf.at[far, pl.ds(cut, rows - cut)], xq.at[i, 3])

    slot = lax.broadcasted_iota(jnp.int32, (CAP, TOK), 0).astype(F32)

    def places(match):
        before = (
            lax.broadcasted_iota(jnp.int32, (TOK, TOK), 0) < lax.broadcasted_iota(jnp.int32, (TOK, TOK), 1)
        )
        upper = jnp.where(before, 1.0, 0.0).astype(BF)
        rank = jnp.dot(match.astype(BF), upper, preferred_element_type=F32)
        return jnp.where(match > 0.5, rank, -1.0)

    def select(i):
        first = (PER * fs).astype(F32)
        rows = []
        for k in range(NX):
            ids = ta[zi(i) * NX + k, pl.ds(TOK, 16), pl.ds(0, TOK)].astype(F32)[:TOP_K]
            for e in range(PER):
                rows.append(jnp.sum(jnp.where(ids == first + e, 1.0, 0.0), axis=0, keepdims=True))
        place = places(jnp.concatenate(rows, axis=0))
        for k in range(NX):
            hot = jnp.concatenate(
                [jnp.where(slot == place[PER * k + e : PER * k + e + 1], 1.0, 0.0) for e in range(PER)], axis=0
            ).astype(BF)
            rows = jnp.dot(hot, ta[zi(i) * NX + k, pl.ds(0, TOK), :], preferred_element_type=F32).astype(BF)
            for e in range(PER):
                xg[i, e, pl.ds(CAP * k, CAP), cols] = rows[CAP * e : CAP * (e + 1)]

    def weigh(i):
        both = ta[zi(i) * NX + x, pl.ds(TOK, 16), pl.ds(0, TOK)].astype(F32)
        ids, weights = both[:TOP_K], both[TOP_K:]
        first = (ROW_EXPERTS * z).astype(F32)
        hits, sums = [], []
        for e in range(ROW_EXPERTS):
            hit = ids == first + e
            hits.append(jnp.sum(jnp.where(hit, 1.0, 0.0), axis=0, keepdims=True))
            sums.append(jnp.sum(jnp.where(hit, weights, 0.0), axis=0, keepdims=True))
        place = places(jnp.concatenate(hits, axis=0))
        for e in range(ROW_EXPERTS):
            wt[i, pl.ds(CAP * e, CAP), :] = jnp.where(slot == place[e : e + 1], sums[e], 0.0).astype(BF)

    def at(buf, i, w, t):
        return buf.at[i, :, :, pl.ds(pl.multiple_of(t * w, w), w)]

    def half(buf, i, w, t, e):
        return buf.at[i, e, :, pl.ds(pl.multiple_of(t * w, w), w)]

    def tp_send(buf, i, w, s, r, b):
        own = at(buf, i, w, tp)
        copy(own, own, s, r.at[0], fs, yp).start()
        copy(own, own, s, r.at[1], fs, ym).start()
        copy(own, own, s, b, fs, sib).start()

    def tp_pass(buf, i, w, s, r, b):
        a = at(buf, i, w, ym)
        arrived(a, r.at[0])
        h = half(buf, i, w, ym, 0)
        copy(h, h, s, r.at[2], fs, yp).start()
        copy(a, a, s, b, fs, sib).start()
        a = at(buf, i, w, yp)
        arrived(a, r.at[1])
        h = half(buf, i, w, yp, 1)
        copy(h, h, s, r.at[3], fs, ym).start()
        copy(a, a, s, b, fs, sib).start()

    def tp_last(buf, i, w, s, r, b):
        far = tpn(2, 0)
        for e in range(2):
            h = half(buf, i, w, far, e)
            arrived(h, r.at[2 + e])
            copy(h, h, s, b, fs, sib).start()

    def tp_done(buf, i, w, b):
        arrived(buf.at[i, :, :, pl.ds(0, 4 * w)], b)

    peers = [(dz, dx) for dx in (0, 1, 3, 2) for dz in (1, -1, 2, -2, 3, -3, 4, 0)]
    peers = [p for p in peers if p != (0, 0)]
    gu_rows = pl.ds(pl.multiple_of(fs * KR, KR), KR)
    dn_rows = pl.ds(pl.multiple_of(fs * KD, KD), KD)

    def send_gu(n):
        f = fsn(*peers[n])
        copy(wgu.at[f], gu.at[:, gu_rows, :], ss.at[3], er.at[0], f, tp).start()

    def send_dn(n):
        f = fsn(*peers[n])
        copy(wdn.at[f], dn.at[:, dn_rows, :], ss.at[4], er.at[1], f, tp).start()

    def round_weights():
        for load in loads:
            load.wait()

        @pl.loop(0, NF)
        def _(f):
            for e in range(PER):
                wgu[f, e, :, :HC] = (fg[PER * f + e] * gain).astype(BF)
                wgu[f, e, :, HC:] = (fu[PER * f + e] * gain).astype(BF)
                wdn[f, e] = fd[PER * f + e].astype(BF)

        gu[:, gu_rows, :] = wgu[fs]
        dn[:, dn_rows, :] = wdn[fs]

    def gate_up(i):
        for e in range(PER):
            both = jnp.dot(xg[i, e], gu[e], preferred_element_type=F32)
            hg[i, e, :, hcols] = silu_mul(both[:, :HC], both[:, HC:]).astype(BF)

    def shared_gate_up():
        both = jnp.dot(nfull[...], tb[:, pl.ds(0, KR), :].reshape(D, 2 * HC), preferred_element_type=F32)
        mid = silu_mul(both[:, :HC], both[:, HC:]).astype(BF)
        hs[0, 0, :, hcols] = mid[: TOK // 2]
        hs[0, 1, :, hcols] = mid[TOK // 2 :]

    def down(i):
        for e in range(PER):
            out = jnp.dot(hg[i, e], dn[e], preferred_element_type=F32).astype(BF)
            for k in range(NX):
                og[i, k, pl.ds(CAP * e, CAP), :] = out[CAP * k : CAP * (k + 1)]

    def give_x(i):
        r1[i, x] = og[i, x]
        for dx in (1, 3, 2):
            k = lax.rem(x + dx, NX)
            copy(og.at[i, k], r1.at[i, x], ss.at[5], d1.at[i], fsn(0, dx), tp).start()

    def give_z(i):
        arrived(r1.at[i, pl.ds(0, NX - 1)], d1.at[i])
        part = lax.dot_general(
            wt[i], r1[i].reshape(NX * PER * CAP, DC), (((0,), (0,)), ((), ())), preferred_element_type=F32
        ).astype(BF)
        if i == 0:
            pr[z] = part
        else:
            pt[i] = part
            copy(pt.at[i], pr.at[z], ss.at[7], dr.at[0], zi(i) * NX + x, tp).start()

    tok = lambda i: (ta, i, ss.at[0], zr, xr)
    shr = lambda i: (tb, i, ss.at[8], szr, sxr)
    bq = lambda i: (xg, i, DC, ss.at[1], br.at[i], bs.at[i])
    cq = lambda i: (hg, i, HC, ss.at[2], cr.at[i], cs.at[i])
    shared = (hs, 0, HC, ss.at[6], cr.at[NZ], cs.at[NZ])
    outs = []

    def put(src, dst):
        outs.append(pltpu.make_async_copy(src, dst, lo.at[len(outs)]))
        outs[-1].start()

    def shared_gather(n):
        if 0 <= n < NZ:
            z_step(*shr(n))
        if 0 <= n - 1 < NZ:
            x_step(*shr(n - 1))
        if 0 <= n - 2 < NZ:
            x_last(*shr(n - 2))

    todo_gu, todo_dn = list(range(NF - 1)), list(range(NF - 1))
    FIRST = NZ + 4
    for tick in range(FIRST):
        if tick < NZ:
            z_step(*tok(tick))
        if 0 <= tick - 1 < NZ:
            x_step(*tok(tick - 1))
        if 0 <= tick - 2 < NZ:
            x_last(*tok(tick - 2))
            select(tick - 2)
            tp_send(*bq(tick - 2))
        if 0 <= tick - 3 < NZ:
            tp_pass(*bq(tick - 3))
        if 0 <= tick - 4 < NZ:
            tp_last(*bq(tick - 4))
        if tick == 0:
            round_weights()
        shared_gather(tick - NZ)
        for _ in range(3 if tick < NZ else 4):
            if todo_gu:
                send_gu(todo_gu.pop(0))
        if tick >= NZ + 2:
            for _ in range(8):
                if todo_dn:
                    send_dn(todo_dn.pop(0))
        if tick < NZ:
            weigh(tick)

    arrived(gu.at[:, pl.ds(0, D - KR), :], er.at[0])
    put(gu.at[:, :, pl.ds(0, HC)], gate_o)
    put(gu.at[:, :, pl.ds(HC, HC)], up_o)
    for tick in range(NZ + 5):
        if tick < NZ:
            i = ORDER[tick]
            tp_done(xg, i, DC, bs.at[i])
            gate_up(i)
            tp_send(*cq(i))
        if 0 <= tick - 1 < NZ:
            tp_pass(*cq(ORDER[tick - 1]))
        if 0 <= tick - 2 < NZ:
            tp_last(*cq(ORDER[tick - 2]))
        for _ in range(8):
            if todo_dn:
                send_dn(todo_dn.pop(0))
        n = tick + FIRST - NZ
        shared_gather(n)
        if n == NZ + 2:
            shared_gate_up()
            tp_send(*shared)
            put(tb.at[:, pl.ds(0, KR), pl.ds(0, HC)], sg_o)
            put(tb.at[:, pl.ds(0, KR), pl.ds(HC, HC)], su_o)
            put(tb.at[:, pl.ds(KR, KD), :], sd_o)
        elif n == NZ + 3:
            tp_pass(*shared)
        elif n == NZ + 4:
            tp_last(*shared)
        if 0 <= tick - 3 < NZ:
            i = ORDER[tick - 3]
            if tick == 3:
                arrived(dn.at[:, pl.ds(0, DE - KD), :], er.at[1])
                put(dn, dn_o)
            tp_done(hg, i, HC, cs.at[i])
            down(i)
            give_x(i)
        if 0 <= tick - 4 < NZ:
            give_z(ORDER[tick - 4])
    tp_done(hs, 0, HC, cs.at[NZ])
    sdn = tb[:, pl.ds(KR, KD), :].reshape(DE, DC)
    total = jnp.concatenate([jnp.dot(hs[0, e], sdn, preferred_element_type=F32) for e in range(2)], axis=0)
    arrived(pr.at[pl.ds(0, NZ - 1)], dr.at[0])
    for k in range(NZ):
        total = total + pr[k].astype(F32)
    mv[...] = total.astype(BF)
    put(mv, mixed_o)

    def sent(ref, s):
        copy(ref, ref, s, dr.at[0], fs, sib).wait_send()

    sent(ta.at[pl.ds(0, NF - 1)], ss.at[0])
    sent(tb.at[pl.ds(0, NF - 1)], ss.at[8])
    sent(xg.at[pl.ds(0, NZ - 1)], ss.at[1])
    sent(hg.at[pl.ds(0, NZ - 1)], ss.at[2])
    sent(gu.at[:, pl.ds(0, D - KR), :], ss.at[3])
    sent(dn.at[:, pl.ds(0, DE - KD), :], ss.at[4])
    sent(r1.at[:, pl.ds(0, NX - 1)], ss.at[5])
    sent(hs.at[0, :, :, pl.ds(0, 7 * HC)], ss.at[6])
    sent(pr.at[pl.ds(0, NZ - 1)], ss.at[7])
    for out in outs:
        out.wait()


def exchange(tokens, ids, rw, gain, sgate, sup, sdown, gate, up, down_w):
    vmem, anyw = pl.BlockSpec(memory_space=pltpu.VMEM), pl.BlockSpec(memory_space=pl.ANY)
    dma = pltpu.SemaphoreType.DMA
    return pl.pallas_call(
        kernel,
        out_shape=(
            jax.ShapeDtypeStruct((PER, D, HC), BF),
            jax.ShapeDtypeStruct((PER, D, HC), BF),
            jax.ShapeDtypeStruct((PER, DE, DC), BF),
            jax.ShapeDtypeStruct((NF, KR, HC), BF),
            jax.ShapeDtypeStruct((NF, KR, HC), BF),
            jax.ShapeDtypeStruct((NF, KD, DC), BF),
            jax.ShapeDtypeStruct((TOK, DC), BF),
        ),
        in_specs=[vmem] * 7 + [anyw] * 3,
        out_specs=(anyw,) * 7,
        scratch_shapes=[
            pltpu.VMEM((EXPERTS, KR, HC), F32),
            pltpu.VMEM((EXPERTS, KR, HC), F32),
            pltpu.VMEM((EXPERTS, KD, DC), F32),
            pltpu.VMEM((NF, PER, KR, 2 * HC), BF),
            pltpu.VMEM((NF, PER, KD, DC), BF),
            pltpu.VMEM((TOK, D), BF),
            pltpu.VMEM((NF, TOK + 16, DC), BF),
            pltpu.VMEM((NF, KR + KD, DC), BF),
            pltpu.VMEM((NZ, PER, SRC, D), BF),
            pltpu.VMEM((PER, D, 2 * HC), BF),
            pltpu.VMEM((PER, DE, DC), BF),
            pltpu.VMEM((NZ, PER, SRC, DE), BF),
            pltpu.VMEM((1, 2, TOK // 2, DE), BF),
            pltpu.VMEM((NZ, NX, PER * CAP, DC), BF),
            pltpu.VMEM((NZ, ROW_EXPERTS * CAP, TOK), BF),
            pltpu.VMEM((NZ, NX, PER * CAP, DC), BF),
            pltpu.VMEM((NZ, TOK, DC), BF),
            pltpu.VMEM((NZ, TOK, DC), BF),
            pltpu.VMEM((TOK, DC), BF),
            dma((9,)), dma((NZ, 4)), dma((9,)), dma((NZ, 4)), dma((NZ, 4)), dma((NZ,)), dma((NZ + 1, 4)),
            dma((NZ + 1,)), dma((2,)), dma((NZ,)), dma((1,)), dma((9,)), dma((7,)), dma((3,)),
        ],
        compiler_params=pltpu.CompilerParams(
            collective_id=0, has_side_effects=True, vmem_limit_bytes=60 * 1024 * 1024
        ),
    )(tokens, ids, rw, gain, sgate, sup, sdown, gate, up, down_w)


def writer(*refs):
    n = len(refs) // 2
    sems = refs[-1]
    copies = [pltpu.make_async_copy(a, b, sems.at[k]) for k, (a, b) in enumerate(zip(refs[:n], refs[n : 2 * n]))]
    for one in copies:
        one.start()
    for one in copies:
        one.wait()


def write_out(*arrays):
    return pl.pallas_call(
        writer,
        out_shape=tuple(jax.ShapeDtypeStruct(a.shape, a.dtype) for a in arrays),
        in_specs=[pl.BlockSpec(memory_space=pltpu.VMEM)] * len(arrays),
        out_specs=(pl.BlockSpec(memory_space=pl.ANY),) * len(arrays),
        scratch_shapes=[pltpu.SemaphoreType.DMA((len(arrays),))],
        compiler_params=pltpu.CompilerParams(vmem_limit_bytes=8 * 1024 * 1024),
    )(*arrays)


def body(
    tokens,
    norm_gain,
    expert_gate,
    expert_up,
    expert_down,
    shared_gate,
    shared_up,
    shared_down,
    expert_ids,
    route_weights,
):
    results = exchange(
        tokens, expert_ids.T, route_weights.T, norm_gain[None], shared_gate, shared_up, shared_down,
        expert_gate, expert_up, expert_down,
    )
    gate_ready, up_ready, down_ready, sg, su, sd, mixed = write_out(*results)
    return (
        gate_ready,
        up_ready,
        down_ready,
        sg.reshape(D, HC),
        su.reshape(D, HC),
        sd.reshape(DE, DC),
        mixed,
    )


def solution(mesh):
    in_specs = (
        P("fs", None),
        P("fs"),
        P(None, "fs", "tp"),
        P(None, "fs", "tp"),
        P(None, "fs", "tp"),
        P("fs", "tp"),
        P("fs", "tp"),
        P("fs", "tp"),
        P("fs", None),
        P("fs", None),
    )
    out_specs = (
        P("fs", None, "tp"),
        P("fs", None, "tp"),
        P("fs", None, "tp"),
        P(None, "tp"),
        P(None, "tp"),
        P(None, "tp"),
        P("fs", "tp"),
    )
    return jax.shard_map(body, mesh=mesh, in_specs=in_specs, out_specs=out_specs, check_vma=False)
```

time: 182 us -> 150 us (0.82); the launches traced: 182 us -> 147 us
  Pallas kernels: 161 us -> 139 us
  other arithmetic: 10.5 us -> 0 us
  matrix products: 3.7 us -> 0 us
  local copies, waits for them, and re-layouts: 5.32 us -> 7.68 us
    pallas_call x1 -> x2, Pallas kernels: 161 us -> 139 us  [the longest x1 137 us: exchange(): pl.pallas_call(kernel, out_shape=(jax.ShapeDtypeStruct((PER, D, HC), BF),...]
    unnamed x29 -> x14, local copies, waits for them, and re-layouts: 1.53 us -> 7.68 us
    convert_element_type x6 -> x0, other arithmetic: 4.19 us -> none  [the longest x1 1.33 us: body(): (wide * lax.rsqrt(jnp.mean(wide * wide, axis=-1, keepdims=True) + EPS)).a...]
    slice x3 -> x0, local copies, waits for them, and re-layouts: 3.77 us -> none  [the longest x1 1.68 us: body(): gu[:, :, HC:]]
    dot_general x3 -> x0, matrix products: 3.7 us -> none  [the longest x1 2.14 us: body(): jnp.dot(high, rows, preferred_element_type=F32)]
    concatenate x2 -> x0, other arithmetic: 2.43 us -> none  [the longest x1 1.7 us: body(): jnp.concatenate([expert_gate * gain, expert_up * gain], axis=2).astype(BF)]
    another operation x1 -> x0, other arithmetic: 2.19 us -> none
where the time goes in v2:
time: 150 us; the launch traced here: 147 us
  Pallas kernels  139 us (93%)
  local copies, waits for them, and re-layouts  7.68 us (5%)
    pallas_call x1, Pallas kernels, exchange(): pl.pallas_call(kernel, out_shape=(jax.ShapeDtypeStruct((PER, D, HC), BF),...  137 us
    unnamed x14, local copies, waits for them, and re-layouts  7.68 us

profile of v2, /device:TPU:8, one launch (start us, length us, event | category | flops | bytes accessed | tf_op | source)
XLA Modules:
  0.0 147.2 jit_solution(15660367442294413150)
XLA Ops:
  0.6 136.7 %shard_map.153 = (bf16[2,2048,128]{2,1,0:T(8,128)(2,1)}, bf16[2,2048,128]{2,1,0:T(8,128)(2,1)}, bf16[2,1024,256]{2,1,0:T(8,128)(2,1)}, bf16[32,64,128]{2,1,0:T(8...) custom-call(bf16[192,2048]{1,0:T(8,128)(2,1)} %tokens.1, ...), custom_call_target="tpu_custom_call" | custom-call | tf_op jit(solution)/shard_map/pallas_call | solution.py:376
  137.3 0.0 copy-start
  137.3 1.2 copy-done
  138.5 0.0 copy-start.1
  138.5 1.2 copy-done.1
  139.8 0.0 copy-start.2
  139.8 1.2 copy-done.2
  141.0 0.0 copy-start.3
  141.0 1.0 copy-done.3
  142.0 0.0 copy-start.4
  142.0 1.0 copy-done.4
  143.1 0.0 copy-start.5
  143.1 1.0 copy-done.5
  144.1 0.0 copy-start.6
  144.1 0.9 copy-done.6
  145.0 2.2 %shard_map.154 = (bf16[2,2048,128]{2,1,0:T(8,128)(2,1)}, bf16[2,2048,128]{2,1,0:T(8,128)(2,1)}, bf16[2,1024,256]{2,1,0:T(8,128)(2,1)}, bf16[32,64,128]{2,1,0:T(8...) custom-call(bf16[2,2048,128]{2,1,0:T(8,128)(2,1)S(1)} %copy-done, ...), custom_call_target="tpu_custom_call" | custom-call | tf_op jit(solution)/shard_map/pallas_call | solution.py:429
Async XLA Ops:
  137.3 1.2 copy-start
  138.5 1.2 copy-start.1
  139.8 1.2 copy-start.2
  141.0 1.0 copy-start.3
  142.0 1.0 copy-start.4
  143.1 1.0 copy-start.5
  144.1 0.9 copy-start.6

commit v3 on v2

--- a/solution.py
+++ b/solution.py
@@ -17,7 +17,11 @@
 SRC = NX * CAP
 ROW_EXPERTS = NX * PER
 OFFS = (0, -1, 1, -2, 2, -3, 3, 4)
-ORDER = (4, 3, 6, 5, 7, 2, 1, 0)
+ORDER = (5, 7, 3, 6, 1, 4, 0, 2)
+SECOND = 10
+SHARED = 6
+LAG = 3
+FEED = (1, 1, 1, 1, 0)
 BF, F32 = jnp.bfloat16, jnp.float32
 MESH = pl.DeviceIdType.MESH
 
@@ -28,9 +32,9 @@
 
 def kernel(
     tokens, ids_in, rw_in, gain_in, sgate, sup, sdown, gate, up, down_w,
-    gate_o, up_o, dn_o, sg_o, su_o, sd_o, mixed_o,
-    fg, fu, fd, wgu, wdn, nfull, ta, tb, xg, gu, dn, hg, hs, og, wt, r1, pt, pr, mv,
-    zr, xr, szr, sxr, br, bs, cr, cs, er, d1, dr, ss, lo, li,
+    gu, dn, tb, mv,
+    fg, fu, fd, wgu, wdn, nfull, ta, xg, hg, hs, og, wt, r1, pt, pr, po, sh,
+    zr, xr, szr, sxr, br, bs, cr, cs, er, d1, dr, ss, li,
 ):
     fs, tp = lax.axis_index("fs"), lax.axis_index("tp")
     z, x = fs // NX, lax.rem(fs, NX)
@@ -199,7 +203,8 @@
     def tp_done(buf, i, w, b):
         arrived(buf.at[i, :, :, pl.ds(0, 4 * w)], b)
 
-    peers = [(dz, dx) for dx in (0, 1, 3, 2) for dz in (1, -1, 2, -2, 3, -3, 4, 0)]
+    zs = (1, -1, 2, -2, 3, -3, 4, 0)
+    peers = [(zs[(a + 2 * b) % NZ], (0, 1, 3, 2)[b]) for a in range(NZ) for b in range(NX)]
     peers = [p for p in peers if p != (0, 0)]
     gu_rows = pl.ds(pl.multiple_of(fs * KR, KR), KR)
     dn_rows = pl.ds(pl.multiple_of(fs * KD, KD), KD)
@@ -253,23 +258,24 @@
         arrived(r1.at[i, pl.ds(0, NX - 1)], d1.at[i])
         part = lax.dot_general(
             wt[i], r1[i].reshape(NX * PER * CAP, DC), (((0,), (0,)), ((), ())), preferred_element_type=F32
-        ).astype(BF)
-        if i == 0:
-            pr[z] = part
-        else:
-            pt[i] = part
-            copy(pt.at[i], pr.at[z], ss.at[7], dr.at[0], zi(i) * NX + x, tp).start()
+        )
+        d = OFFS[i]
+        if d == 0:
+            po[...] = part
+            return
+        far, base = (4, 0) if d > 0 else (3, 4)
+        k = base + abs(d)
+        if abs(d) < far:
+            arrived(pr.at[k], dr.at[k])
+            part = part + pr[k].astype(F32)
+        pt[i] = part.astype(BF)
+        copy(pt.at[i], pr.at[k - 1], ss.at[7], dr.at[k - 1], zp if d > 0 else zm, tp).start()
 
     tok = lambda i: (ta, i, ss.at[0], zr, xr)
     shr = lambda i: (tb, i, ss.at[8], szr, sxr)
     bq = lambda i: (xg, i, DC, ss.at[1], br.at[i], bs.at[i])
     cq = lambda i: (hg, i, HC, ss.at[2], cr.at[i], cs.at[i])
     shared = (hs, 0, HC, ss.at[6], cr.at[NZ], cs.at[NZ])
-    outs = []
-
-    def put(src, dst):
-        outs.append(pltpu.make_async_copy(src, dst, lo.at[len(outs)]))
-        outs[-1].start()
 
     def shared_gather(n):
         if 0 <= n < NZ:
@@ -279,80 +285,80 @@
         if 0 <= n - 2 < NZ:
             x_last(*shr(n - 2))
 
-    todo_gu, todo_dn = list(range(NF - 1)), list(range(NF - 1))
-    FIRST = NZ + 4
-    for tick in range(FIRST):
+    todo = [(send_gu, n) for n in range(NF - 1)] + [(send_dn, n) for n in range(NF - 1)]
+
+    def flush(keep):
+        while len(todo) > keep:
+            send, n = todo.pop(0)
+            send(n)
+
+    def feed(k):
+        flush(len(todo) - min(FEED[k] if len(todo) >= NF else 2 * FEED[k], len(todo)))
+
+    for tick in range(SECOND + NZ + LAG + 2):
         if tick < NZ:
             z_step(*tok(tick))
+        if tick == 0:
+            round_weights()
+        feed(0)
         if 0 <= tick - 1 < NZ:
             x_step(*tok(tick - 1))
+        feed(1)
         if 0 <= tick - 2 < NZ:
             x_last(*tok(tick - 2))
             select(tick - 2)
             tp_send(*bq(tick - 2))
+        feed(2)
         if 0 <= tick - 3 < NZ:
             tp_pass(*bq(tick - 3))
+        feed(3)
         if 0 <= tick - 4 < NZ:
             tp_last(*bq(tick - 4))
-        if tick == 0:
-            round_weights()
-        shared_gather(tick - NZ)
-        for _ in range(3 if tick < NZ else 4):
-            if todo_gu:
-                send_gu(todo_gu.pop(0))
-        if tick >= NZ + 2:
-            for _ in range(8):
-                if todo_dn:
-                    send_dn(todo_dn.pop(0))
+        feed(4)
+        shared_gather(tick - SHARED)
         if tick < NZ:
             weigh(tick)
-
-    arrived(gu.at[:, pl.ds(0, D - KR), :], er.at[0])
-    put(gu.at[:, :, pl.ds(0, HC)], gate_o)
-    put(gu.at[:, :, pl.ds(HC, HC)], up_o)
-    for tick in range(NZ + 5):
-        if tick < NZ:
-            i = ORDER[tick]
+        t = tick - SECOND
+        if t == 0:
+            flush(NF - 1)
+            arrived(gu.at[:, pl.ds(0, D - KR), :], er.at[0])
+        if 0 <= t < NZ:
+            i = ORDER[t]
             tp_done(xg, i, DC, bs.at[i])
             gate_up(i)
             tp_send(*cq(i))
-        if 0 <= tick - 1 < NZ:
-            tp_pass(*cq(ORDER[tick - 1]))
-        if 0 <= tick - 2 < NZ:
-            tp_last(*cq(ORDER[tick - 2]))
-        for _ in range(8):
-            if todo_dn:
-                send_dn(todo_dn.pop(0))
-        n = tick + FIRST - NZ
-        shared_gather(n)
-        if n == NZ + 2:
+        if 0 <= t - 1 < NZ:
+            tp_pass(*cq(ORDER[t - 1]))
+        if 0 <= t - 2 < NZ:
+            tp_last(*cq(ORDER[t - 2]))
+        n = tick - SHARED - NZ
+        if n == 2:
             shared_gate_up()
             tp_send(*shared)
-            put(tb.at[:, pl.ds(0, KR), pl.ds(0, HC)], sg_o)
-            put(tb.at[:, pl.ds(0, KR), pl.ds(HC, HC)], su_o)
-            put(tb.at[:, pl.ds(KR, KD), :], sd_o)
-        elif n == NZ + 3:
+        elif n == 3:
             tp_pass(*shared)
-        elif n == NZ + 4:
+        elif n == 4:
             tp_last(*shared)
-        if 0 <= tick - 3 < NZ:
-            i = ORDER[tick - 3]
-            if tick == 3:
+        if 0 <= t - LAG < NZ:
+            i = ORDER[t - LAG]
+            if t == LAG:
+                flush(0)
                 arrived(dn.at[:, pl.ds(0, DE - KD), :], er.at[1])
-                put(dn, dn_o)
             tp_done(hg, i, HC, cs.at[i])
             down(i)
             give_x(i)
-        if 0 <= tick - 4 < NZ:
-            give_z(ORDER[tick - 4])
-    tp_done(hs, 0, HC, cs.at[NZ])
-    sdn = tb[:, pl.ds(KR, KD), :].reshape(DE, DC)
-    total = jnp.concatenate([jnp.dot(hs[0, e], sdn, preferred_element_type=F32) for e in range(2)], axis=0)
-    arrived(pr.at[pl.ds(0, NZ - 1)], dr.at[0])
-    for k in range(NZ):
+        if 0 <= t - LAG - 1 < NZ:
+            give_z(ORDER[t - LAG - 1])
+        if t == NZ + 1:
+            tp_done(hs, 0, HC, cs.at[NZ])
+            sdn = tb[:, pl.ds(KR, KD), :].reshape(DE, DC)
+            for e in range(2):
+                sh[pl.ds(e * (TOK // 2), TOK // 2), :] = jnp.dot(hs[0, e], sdn, preferred_element_type=F32)
+    total = sh[...] + po[...]
+    for k in (4, 0):
+        arrived(pr.at[k], dr.at[k])
         total = total + pr[k].astype(F32)
     mv[...] = total.astype(BF)
-    put(mv, mixed_o)
 
     def sent(ref, s):
         copy(ref, ref, s, dr.at[0], fs, sib).wait_send()
@@ -366,8 +372,6 @@
     sent(r1.at[:, pl.ds(0, NX - 1)], ss.at[5])
     sent(hs.at[0, :, :, pl.ds(0, 7 * HC)], ss.at[6])
     sent(pr.at[pl.ds(0, NZ - 1)], ss.at[7])
-    for out in outs:
-        out.wait()
 
 
 def exchange(tokens, ids, rw, gain, sgate, sup, sdown, gate, up, down_w):
@@ -376,16 +380,13 @@
     return pl.pallas_call(
         kernel,
         out_shape=(
-            jax.ShapeDtypeStruct((PER, D, HC), BF),
-            jax.ShapeDtypeStruct((PER, D, HC), BF),
-            jax.ShapeDtypeStruct((PER, DE, DC), BF),
-            jax.ShapeDtypeStruct((NF, KR, HC), BF),
-            jax.ShapeDtypeStruct((NF, KR, HC), BF),
-            jax.ShapeDtypeStruct((NF, KD, DC), BF),
-            jax.ShapeDtypeStruct((TOK, DC), BF),
+            pltpu.VMEM((PER, D, 2 * HC), BF),
+            pltpu.VMEM((PER, DE, DC), BF),
+            pltpu.VMEM((NF, KR + KD, DC), BF),
+            pltpu.VMEM((TOK, DC), BF),
         ),
         in_specs=[vmem] * 7 + [anyw] * 3,
-        out_specs=(anyw,) * 7,
+        out_specs=(vmem,) * 4,
         scratch_shapes=[
             pltpu.VMEM((EXPERTS, KR, HC), F32),
             pltpu.VMEM((EXPERTS, KR, HC), F32),
@@ -394,31 +395,37 @@
             pltpu.VMEM((NF, PER, KD, DC), BF),
             pltpu.VMEM((TOK, D), BF),
             pltpu.VMEM((NF, TOK + 16, DC), BF),
-            pltpu.VMEM((NF, KR + KD, DC), BF),
             pltpu.VMEM((NZ, PER, SRC, D), BF),
-            pltpu.VMEM((PER, D, 2 * HC), BF),
-            pltpu.VMEM((PER, DE, DC), BF),
             pltpu.VMEM((NZ, PER, SRC, DE), BF),
             pltpu.VMEM((1, 2, TOK // 2, DE), BF),
             pltpu.VMEM((NZ, NX, PER * CAP, DC), BF),
             pltpu.VMEM((NZ, ROW_EXPERTS * CAP, TOK), BF),
             pltpu.VMEM((NZ, NX, PER * CAP, DC), BF),
             pltpu.VMEM((NZ, TOK, DC), BF),
-            pltpu.VMEM((NZ, TOK, DC), BF),
-            pltpu.VMEM((TOK, DC), BF),
+            pltpu.VMEM((NZ - 1, TOK, DC), BF),
+            pltpu.VMEM((TOK, DC), F32),
+            pltpu.VMEM((TOK, DC), F32),
             dma((9,)), dma((NZ, 4)), dma((9,)), dma((NZ, 4)), dma((NZ, 4)), dma((NZ,)), dma((NZ + 1, 4)),
-            dma((NZ + 1,)), dma((2,)), dma((NZ,)), dma((1,)), dma((9,)), dma((7,)), dma((3,)),
+            dma((NZ + 1,)), dma((2,)), dma((NZ,)), dma((NZ - 1,)), dma((9,)), dma((3,)),
         ],
         compiler_params=pltpu.CompilerParams(
-            collective_id=0, has_side_effects=True, vmem_limit_bytes=60 * 1024 * 1024
+            collective_id=0, has_side_effects=True, vmem_limit_bytes=54 * 1024 * 1024
         ),
     )(tokens, ids, rw, gain, sgate, sup, sdown, gate, up, down_w)
 
 
-def writer(*refs):
-    n = len(refs) // 2
-    sems = refs[-1]
-    copies = [pltpu.make_async_copy(a, b, sems.at[k]) for k, (a, b) in enumerate(zip(refs[:n], refs[n : 2 * n]))]
+def writer(gu, dn, tb, mv, gate_o, up_o, dn_o, sg_o, su_o, sd_o, mixed_o, sems):
+    left, right = pl.ds(0, HC), pl.ds(HC, HC)
+    pairs = (
+        (gu.at[:, :, left], gate_o),
+        (gu.at[:, :, right], up_o),
+        (dn, dn_o),
+        (tb.at[:, pl.ds(0, KR), left], sg_o),
+        (tb.at[:, pl.ds(0, KR), right], su_o),
+        (tb.at[:, pl.ds(KR, KD), :], sd_o),
+        (mv, mixed_o),
+    )
+    copies = [pltpu.make_async_copy(a, b, sems.at[k]) for k, (a, b) in enumerate(pairs)]
     for one in copies:
         one.start()
     for one in copies:
@@ -426,12 +433,13 @@
 
 
 def write_out(*arrays):
+    shapes = ((PER, D, HC), (PER, D, HC), (PER, DE, DC), (NF, KR, HC), (NF, KR, HC), (NF, KD, DC), (TOK, DC))
     return pl.pallas_call(
         writer,
-        out_shape=tuple(jax.ShapeDtypeStruct(a.shape, a.dtype) for a in arrays),
+        out_shape=tuple(jax.ShapeDtypeStruct(s, BF) for s in shapes),
         in_specs=[pl.BlockSpec(memory_space=pltpu.VMEM)] * len(arrays),
-        out_specs=(pl.BlockSpec(memory_space=pl.ANY),) * len(arrays),
-        scratch_shapes=[pltpu.SemaphoreType.DMA((len(arrays),))],
+        out_specs=(pl.BlockSpec(memory_space=pl.ANY),) * len(shapes),
+        scratch_shapes=[pltpu.SemaphoreType.DMA((len(shapes),))],
         compiler_params=pltpu.CompilerParams(vmem_limit_bytes=8 * 1024 * 1024),
     )(*arrays)
 

time: 150 us -> 137 us (0.913); the launches traced: 147 us -> 137 us
  local copies, waits for them, and re-layouts: 7.68 us -> 0 us
  Pallas kernels: 139 us -> 136 us
    unnamed x14 -> x0, local copies, waits for them, and re-layouts: 7.68 us -> none
    pallas_call x2, Pallas kernels: 139 us -> 136 us  [the longest x1 134 us: exchange(): pl.pallas_call(kernel, out_shape=(pltpu.VMEM((PER, D, 2 * HC), BF), pltpu...]
where the time goes in v3:
time: 137 us
  Pallas kernels  136 us (99%)
    pallas_call x1, Pallas kernels, exchange(): pl.pallas_call(kernel, out_shape=(pltpu.VMEM((PER, D, 2 * HC), BF), pltpu...  134 us

profile of v3, /device:TPU:8, one launch (start us, length us, event | category | flops | bytes accessed | tf_op | source)
XLA Modules:
  0.0 136.8 jit_solution(8908182681518711069)
XLA Ops:
  0.6 134.0 %shard_map.153 = (bf16[2,2048,256]{2,1,0:T(8,128)(2,1)S(1)}, bf16[2,1024,256]{2,1,0:T(8,128)(2,1)S(1)}, bf16[32,96,256]{2,1,0:T(8,128)(2,1)S(1)}, bf16[192,256]{1,0:T(8,128)(2,1)S(1)}) custom-call(bf16[192,2048]{1,0:T(8,128)(2,1)} %tokens.1, s32[8,192]{1,0:T(8,128)} %bitcast.6, f32[8,192]{1,0:T(8,128)} %bitcast.7, f32[1,64]{1,0:T(1,128)} %bitcast.8, ...), custom_call_target="tpu_custom_call" | custom-call | tf_op jit(solution)/shard_map/pallas_call | solution.py:380
  134.6 2.2 %shard_map.154 = (bf16[2,2048,128]{2,1,0:T(8,128)(2,1)}, bf16[2,2048,128]{2,1,0:T(8,128)(2,1)}, bf16[2,1024,256]{2,1,0:T(8,128)(2,1)}, bf16[32,64,128]{2,1,0:T(8...) custom-call(bf16[2,2048,256]{2,1,0:T(8,128)(2,1)S(1)} %get-tuple-element.18.gu, ...), custom_call_target="tpu_custom_call" | custom-call | tf_op jit(solution)/shard_map/pallas_call | solution.py:437

commit v4 on v3

--- a/solution.py
+++ b/solution.py
@@ -31,8 +31,9 @@
 
 
 def kernel(
-    tokens, ids_in, rw_in, gain_in, sgate, sup, sdown, gate, up, down_w,
+    tokens_h, ids_h, rw_h, gain_h, sgate_h, sup_h, sdown_h, gate, up, down_w,
     gu, dn, tb, mv,
+    tokens, ids_in, rw_in, gain_in, sgate, sup, sdown,
     fg, fu, fd, wgu, wdn, nfull, ta, xg, hg, hs, og, wt, r1, pt, pr, po, sh,
     zr, xr, szr, sxr, br, bs, cr, cs, er, d1, dr, ss, li,
 ):
@@ -58,8 +59,14 @@
     def arrived(dst, r):
         copy(dst, dst, ss.at[0], r, fs, sib).wait_recv()
 
-    loads = [pltpu.make_async_copy(a, b, li.at[k]) for k, (a, b) in enumerate(((gate, fg), (up, fu), (down_w, fd)))]
-    for load in loads:
+    small = (
+        (tokens_h, tokens), (ids_h, ids_in), (rw_h, rw_in), (gain_h, gain_in),
+        (sgate_h, sgate), (sup_h, sup), (sdown_h, sdown),
+    )
+    large = ((gate, fg), (up, fu), (down_w, fd))
+    copies = [pltpu.make_async_copy(a, b, li.at[k]) for k, (a, b) in enumerate(small + large)]
+    first, loads = copies[: len(small)], copies[len(small) :]
+    for load in copies:
         load.start()
 
     barrier = pltpu.get_barrier_semaphore()
@@ -68,6 +75,8 @@
     for t in (yp, ym, sib):
         pl.semaphore_signal(barrier, inc=1, device_id=(fs, t), device_id_type=MESH)
 
+    for load in first:
+        load.wait()
     wide = tokens[...].astype(F32)
     scale = lax.rsqrt(jnp.mean(wide * wide, axis=-1, keepdims=True) + EPS)
     nfull[...] = (wide * scale).astype(BF)
@@ -293,7 +302,8 @@
             send(n)
 
     def feed(k):
-        flush(len(todo) - min(FEED[k] if len(todo) >= NF else 2 * FEED[k], len(todo)))
+        if tick > 0:
+            flush(len(todo) - min(FEED[k] if len(todo) >= NF else 2 * FEED[k], len(todo)))
 
     for tick in range(SECOND + NZ + LAG + 2):
         if tick < NZ:
@@ -385,9 +395,16 @@
             pltpu.VMEM((NF, KR + KD, DC), BF),
             pltpu.VMEM((TOK, DC), BF),
         ),
-        in_specs=[vmem] * 7 + [anyw] * 3,
+        in_specs=[anyw] * 10,
         out_specs=(vmem,) * 4,
         scratch_shapes=[
+            pltpu.VMEM((TOK, D), BF),
+            pltpu.VMEM((TOP_K, TOK), jnp.int32),
+            pltpu.VMEM((TOP_K, TOK), F32),
+            pltpu.VMEM((1, KR), F32),
+            pltpu.VMEM((KR, HC), F32),
+            pltpu.VMEM((KR, HC), F32),
+            pltpu.VMEM((KD, DC), F32),
             pltpu.VMEM((EXPERTS, KR, HC), F32),
             pltpu.VMEM((EXPERTS, KR, HC), F32),
             pltpu.VMEM((EXPERTS, KD, DC), F32),
@@ -406,7 +423,7 @@
             pltpu.VMEM((TOK, DC), F32),
             pltpu.VMEM((TOK, DC), F32),
             dma((9,)), dma((NZ, 4)), dma((9,)), dma((NZ, 4)), dma((NZ, 4)), dma((NZ,)), dma((NZ + 1, 4)),
-            dma((NZ + 1,)), dma((2,)), dma((NZ,)), dma((NZ - 1,)), dma((9,)), dma((3,)),
+            dma((NZ + 1,)), dma((2,)), dma((NZ,)), dma((NZ - 1,)), dma((9,)), dma((10,)),
         ],
         compiler_params=pltpu.CompilerParams(
             collective_id=0, has_side_effects=True, vmem_limit_bytes=54 * 1024 * 1024

time: 137 us -> 135 us (0.985)
  Pallas kernels: 136 us -> 134 us
    pallas_call x1, Pallas kernels: 134 us -> 132 us  [exchange(): pl.pallas_call(kernel, out_shape=(pltpu.VMEM((PER, D, 2 * HC), BF), pltpu...]
where the time goes in v4:
time: 135 us
  Pallas kernels  134 us (99%)
    pallas_call x1, Pallas kernels, exchange(): pl.pallas_call(kernel, out_shape=(pltpu.VMEM((PER, D, 2 * HC), BF), pltpu...  132 us

profile of v4, /device:TPU:8, one launch (start us, length us, event | category | flops | bytes accessed | tf_op | source)
XLA Modules:
  0.0 135.1 jit_solution(11636536243957251772)
XLA Ops:
  0.6 132.2 %shard_map.153 = (bf16[2,2048,256]{2,1,0:T(8,128)(2,1)S(1)}, bf16[2,1024,256]{2,1,0:T(8,128)(2,1)S(1)}, bf16[32,96,256]{2,1,0:T(8,128)(2,1)S(1)}, bf16[192,256]{1,0:T(8,128)(2,1)S(1)}) custom-call(bf16[192,2048]{1,0:T(8,128)(2,1)} %tokens_h.1, s32[8,192]{1,0:T(8,128)} %bitcast.6, f32[8,192]{1,0:T(8,128)} %bitcast.7, f32[1,64]{1,0:T(1,128)} %bitcast.8, ...), custom_call_target="tpu_custom_call" | custom-call | tf_op jit(solution)/shard_map/pallas_call | solution.py:390
  132.8 2.2 %shard_map.154 = (bf16[2,2048,128]{2,1,0:T(8,128)(2,1)}, bf16[2,2048,128]{2,1,0:T(8,128)(2,1)}, bf16[2,1024,256]{2,1,0:T(8,128)(2,1)}, bf16[32,64,128]{2,1,0:T(8...) custom-call(bf16[2,2048,256]{2,1,0:T(8,128)(2,1)S(1)} %get-tuple-element.18.gu, ...), custom_call_target="tpu_custom_call" | custom-call | tf_op jit(solution)/shard_map/pallas_call | solution.py:454
